TPU v7x, 128 devices: a whole 4x4x4 slice. The times are simulated.
128 devices in a mesh: rep: 4 (over z), fs: 4 (over y), tp: 8 (over x, core).
Axes of the slice: x: 4, y: 4, z: 4, core: 2. Of those that a mesh axis runs over, the one named last changes fastest.
Arguments:
- tokens_in: bfloat16 [12288, 1024], P(('rep', 'fs', 'tp')), may hold values from -6 to 6
- out_grad: bfloat16 [12288, 1024], P(('rep', 'fs', 'tp')), may hold values from -24 to 24
- gate_weight: bfloat16 [1024, 2816], P('fs', 'tp'), may hold values from -0.1875 to 0.1875
- up_weight: bfloat16 [1024, 2816], P('fs', 'tp'), may hold values from -0.1875 to 0.1875
- down_weight: bfloat16 [2816, 1024], P('tp', 'fs'), may hold values from -0.109375 to 0.109375
Outputs:
- grad_in: bfloat16 [12288, 1024], P(('rep', 'fs', 'tp'))
- grad_gate_w: float32 [1024, 2816], P('fs', 'tp')
- grad_up_w: float32 [1024, 2816], P('fs', 'tp')
- grad_down_w: float32 [2816, 1024], P('tp', 'fs')
All inputs are finite; a program needn't handle non-finite values.
Results may differ from a plain program's by a relative error of at most 0.02.
Values may be sent and summed in bfloat16 or wider, within the bound.
A program may use at most 64 MiB of HBM per device.

v0:
```python
import jax
import jax.numpy as jnp
from jax import lax
from jax.sharding import PartitionSpec as P


def summed_rows(product, width, axis):
    everything = product(jnp.int32(0), lax.axis_size(axis) * width)
    own = lax.psum_scatter(everything.astype(jnp.bfloat16), axis, scatter_dimension=0, tiled=True)
    return own.astype(jnp.float32)


def padded_to(lines, peers):
    spare = -len(lines) % peers
    return jnp.pad(lines, [(0, spare)] + [(0, 0)] * (lines.ndim - 1))


def total_of(x, axis):
    lines = x.reshape(-1, *x.shape[1:][-1:])
    own = lax.psum_scatter(
        padded_to(lines, lax.axis_size(axis)), axis, scatter_dimension=0, tiled=True
    )
    whole = lax.all_gather(own, axis).reshape(-1, *lines.shape[1:])
    return lax.slice_in_dim(whole, 0, len(lines)).reshape(x.shape)


def contract_last(left, right):
    return lax.dot_general(
        left, right, (((1,), (1,)), ((), ())), preferred_element_type=jnp.float32
    )


def contract_first(left, right):
    return lax.dot_general(
        left, right, (((0,), (0,)), ((), ())), preferred_element_type=jnp.float32
    )


def body(tokens_in, out_grad, gate_weight, up_weight, down_weight):
    replicas = lax.axis_size("rep")
    shards = lax.axis_size("fs")
    columns = lax.axis_size("tp")
    local_rows = tokens_in.shape[0]
    model_width = gate_weight.shape[0] * shards
    hidden_cols = gate_weight.shape[1]
    factor = (local_rows * replicas * shards * columns) ** (-0.5)
    gate_full, up_full, down_full = (
        lax.all_gather(gate_weight, "fs", axis=0, tiled=True),
        lax.all_gather(up_weight, "fs", axis=0, tiled=True),
        lax.all_gather(down_weight, "fs", axis=1, tiled=True),
    )
    tokens_all, grads_all = (
        lax.all_gather(tokens_in, "tp", axis=0, tiled=True),
        lax.all_gather(out_grad, "tp", axis=0, tiled=True),
    )
    gate = jnp.dot(tokens_all, gate_full, preferred_element_type=jnp.float32).astype(jnp.bfloat16)
    up_proj = jnp.dot(tokens_all, up_full, preferred_element_type=jnp.float32).astype(jnp.bfloat16)
    gate_wide = gate.astype(jnp.float32)
    up_wide = up_proj.astype(jnp.float32)
    sigmoid = jax.nn.sigmoid(gate_wide)
    activated = gate_wide * sigmoid
    hidden = (activated * up_wide).astype(jnp.bfloat16)
    grad_hidden = contract_last(grads_all, down_full).astype(jnp.bfloat16)
    grad_wide = grad_hidden.astype(jnp.float32)
    grad_gate = (grad_wide * up_wide * sigmoid * (1.0 + gate_wide * (1.0 - sigmoid))).astype(
        jnp.bfloat16
    )
    grad_up = (grad_wide * activated).astype(jnp.bfloat16)

    def input_term(start, count):
        gate_rows = lax.dynamic_slice_in_dim(grad_gate, start, count, 0)
        up_rows = lax.dynamic_slice_in_dim(grad_up, start, count, 0)
        return contract_last(gate_rows, gate_full) + contract_last(up_rows, up_full)

    grad_in = summed_rows(input_term, local_rows, "tp").astype(jnp.bfloat16)

    def weight_term(token_order, grad_order):

        def term(start, count):
            token_cols = lax.dynamic_slice_in_dim(token_order, start, count, 1)
            grad_cols = lax.dynamic_slice_in_dim(grad_order, start, count, 1)
            return factor * jnp.concatenate(
                [
                    contract_first(token_cols, grad_gate),
                    contract_first(token_cols, grad_up),
                    contract_first(grad_cols, hidden),
                ],
                axis=1,
            )

        return term

    owned = summed_rows(weight_term(tokens_all, grads_all), model_width // shards, "fs")
    summed = total_of(owned.astype(jnp.bfloat16), "rep").astype(jnp.float32)
    grad_gate_w = summed[:, :hidden_cols]
    grad_up_w = summed[:, hidden_cols : 2 * hidden_cols]
    grad_down_w = summed[:, 2 * hidden_cols :].T
    return (grad_in, grad_gate_w, grad_up_w, grad_down_w)


def solution(mesh):
    return jax.shard_map(
        body,
        mesh=mesh,
        in_specs=(
            P(("rep", "fs", "tp"), None),
            P(("rep", "fs", "tp"), None),
            P("fs", "tp"),
            P("fs", "tp"),
            P("tp", "fs"),
        ),
        out_specs=(P(("rep", "fs", "tp"), None), P("fs", "tp"), P("fs", "tp"), P("tp", "fs")),
        check_vma=False,
    )
```

profile of v0, /device:TPU:0, one launch (start us, length us, event | category | flops | bytes accessed | tf_op | source)
XLA Modules:
  0.0 167.5 jit_solution(8725800605460358486)
XLA Ops:
  7.2 0.0 copy-start
  7.2 0.0 copy-start.1
  7.2 0.0 all-gather.6.cloned.1.call-start
  7.2 0.7 all-gather.6.cloned.1.call-update
  7.9 0.0 all-gather.4.cloned.1.call-start
  8.0 0.7 all-gather.4.cloned.1.call-update
  8.7 0.0 reduce-scatter.8.cloned.1.call-start
  8.7 14.1 %all_gather.25 = bf16[1024,352]{0,1:T(8,128)(2,1)S(1)} all-gather(bf16[256,352]{0,1:T(8,128)(2,1)} %param.7), channel_id=1, replica_groups=mesh['rep'=4,'fs'=4,'tp'=8] {'fs'}, dimensions={0}, use_global_device_ids=true | all-gather | bytes 901120 | tf_op jit(solution)/shard_map/all_gather | solution.py:48
  22.8 0.0 copy-done
  22.8 13.5 %all_gather.24 = bf16[1024,352]{0,1:T(8,128)(2,1)S(1)} all-gather(bf16[256,352]{0,1:T(8,128)(2,1)S(1)} %copy-done), channel_id=1, replica_groups=mesh['rep'=4,'fs'=4,'tp'=8] {'fs'}, dimensions={0}, use_global_device_ids=true | all-gather | bytes 901120 | tf_op jit(solution)/shard_map/all_gather | solution.py:49
  36.3 0.0 copy-done.1
  36.3 14.3 %all_gather.22 = bf16[352,1024]{1,0:T(8,128)(2,1)S(1)} all-gather(bf16[352,256]{1,0:T(8,128)(2,1)S(1)} %copy-done.1), channel_id=1, replica_groups=mesh['rep'=4,'fs'=4,'tp'=8] {'fs'}, dimensions={1}, use_global_device_ids=true | all-gather | bytes 901120 | tf_op jit(solution)/shard_map/all_gather | solution.py:50
  50.6 0.0 all-gather.6.cloned.1.call-done
  50.6 0.0 copy-start.2
  50.6 2.3 %convolution_convert_fusion = bf16[768,352]{0,1:T(8,128)(2,1)S(1)} fusion(bf16[768,1024]{1,0:T(8,128)(2,1)} %all-gather.6.cloned.1.call-done, bf16[1024,352]{0,1:T(8,128)(2,1)S(1)} %all_gather.25), kind=kOutput, calls=%fused_computation.12 | convolution fusion | flops 553918464 | bytes 2834432 | tf_op jit(solution)/shard_map/dot_general | solution.py:56
  52.9 0.0 copy-done.2
  52.9 1.6 convolution_convert_fusion.1
  54.5 8.4 %all-gather.4.cloned.1.call-done = bf16[768,1024]{1,0:T(8,128)(2,1)} async-done(((bf16[96,1024]{1,0:T(8,128)(2,1)}), bf16[768,1024]{1,0:T(8,128)(2,1)}) %all-gather.4.cloned.1.call-update) | async-done | bytes 1572880 | tf_op jit(solution)/shard_map/all_gather | solution.py:54
  62.8 0.0 copy-start.4
  62.8 0.0 copy-start.5
  62.8 2.3 %convolution_convert_fusion.2 = bf16[768,352]{0,1:T(8,128)(2,1)S(1)} fusion(bf16[768,1024]{1,0:T(8,128)(2,1)} %all-gather.4.cloned.1.call-done, bf16[352,1024]{1,0:T(8,128)(2,1)S(1)} %all_gather.22), kind=kOutput, calls=%fused_computation.14 | convolution fusion | flops 553918464 | bytes 2834432 | tf_op jit(solution)/shard_map/dot_general | solution.py:28
  65.2 0.0 copy-done.4
  65.2 0.0 copy-done.5
  65.2 0.0 copy-start.7
  65.2 0.0 copy-start.3
  65.2 0.8 convolution_bitcast_fusion
  66.0 0.8 copy-done.3
  66.8 1.0 convolution_bitcast_fusion.2
  67.8 0.0 copy-done.7
  67.8 0.8 convolution_bitcast_fusion.1
  68.7 2.0 %fusion = bf16[1024,1056]{0,1:T(8,128)(2,1)} fusion(f32[1024,352]{0,1:T(8,128)S(1)} %convolution_bitcast_fusion, f32[1024,352]{0,1:T(8,128)S(1)} %convolution_bitcast_fusion.1, f32[1024,352]{0,1:T(8,128)S(1)} %convolution_bitcast_fusion.2), kind=kLoop, calls=%fused_computation.1 | loop fusion | flops 4325376 | bytes 6488064 | tf_op jit(solution)/shard_map/convert_element_type | solution.py:9
  70.7 0.0 reduce-scatter.8.cloned.1.call-update
  70.7 0.0 copy-start.6
  70.7 0.0 copy-start.8
  70.7 0.0 reduce-scatter.10.cloned.1.call-start
  70.8 30.6 %reduce-scatter.8.cloned.1.call-done = bf16[256,1056]{0,1:T(8,128)(2,1)} async-done(((bf16[1024,1056]{0,1:T(8,128)(2,1)}), bf16[256,1056]{0,1:T(8,128)(2,1)}) %reduce-scatter.8.cloned.1.call-update) | async-done | bytes 540688 | tf_op jit(solution)/shard_map/reduce_scatter | solution.py:9
  101.3 2.1 %copy.13 = bf16[256,1056]{1,0:T(8,128)(2,1)} copy(bf16[256,1056]{0,1:T(8,128)(2,1)} %reduce-scatter.8.cloned.1.call-done) | data formatting | bytes 1081344
  103.5 0.0 reduce-scatter.10.cloned.1.call-update
  103.5 0.0 reduce-scatter.6.cloned.1.call-start
  103.5 0.0 copy-done.6
  103.5 0.0 copy-done.8
  103.6 1.3 fusion.15
  104.8 2.3 %add_convert_fusion = bf16[768,1024]{1,0:T(8,128)(2,1)} fusion(f32[768,1024]{1,0:T(8,128)S(1)} %fusion.15, bf16[1024,352]{0,1:T(8,128)(2,1)S(1)} %all_gather.24, bf16[768,352]{0,1:T(8,128)(2,1)S(1)} %copy-done.8, bf16[768,352]{0,1:T(8,128)(2,1)S(1)} %convolution_convert_fusion), kind=kOutput, calls=%fused_computation.2 | convolution fusion | flops 557383680 | bytes 6520832 | tf_op jit(solution)/shard_map/dot_general | solution.py:28
  107.2 0.0 reduce-scatter.6.cloned.1.call-update
  107.2 18.3 %reduce-scatter.10.cloned.1.call-done = bf16[64,1056]{1,0:T(8,128)(2,1)} async-done(((bf16[256,1056]{1,0:T(8,128)(2,1)}), bf16[64,1056]{1,0:T(8,128)(2,1)}) %reduce-scatter.10.cloned.1.call-update) | async-done | bytes 135184 | tf_op jit(solution)/shard_map/reduce_scatter | solution.py:20
  125.5 13.1 %all-gather = bf16[256,1056]{1,0:T(8,128)(2,1)S(1)} all-gather(bf16[64,1056]{1,0:T(8,128)(2,1)} %reduce-scatter.10.cloned.1.call-done), channel_id=2, replica_groups=mesh['rep'=4,'fs'=4,'tp'=8] {'rep'}, dimensions={0}, use_global_device_ids=true | all-gather | bytes 675840 | tf_op jit(solution)/shard_map/all_gather | solution.py:23
  138.6 0.1 convert_element_type.57
  138.7 0.1 fusion.17
  138.8 0.9 copy.11
  139.7 0.9 copy.10
  140.6 0.2 slice_bitcast_fusion
  140.8 0.9 copy.12
  141.7 19.3 %reduce-scatter.6.cloned.1.call-done = bf16[96,1024]{1,0:T(8,128)(2,1)} async-done(((bf16[768,1024]{1,0:T(8,128)(2,1)}), bf16[96,1024]{1,0:T(8,128)(2,1)}) %reduce-scatter.6.cloned.1.call-update) | async-done | bytes 196624 | tf_op jit(solution)/shard_map/reduce_scatter | solution.py:9
Async XLA Ops:
  7.2 15.6 %copy-start = (bf16[256,352]{0,1:T(8,128)(2,1)S(1)}, bf16[256,352]{0,1:T(8,128)(2,1)}, u32[]{:S(2)}) copy-start(bf16[256,352]{0,1:T(8,128)(2,1)} %param.8) | copy-start | bytes 540676
  7.2 29.1 %copy-start.1 = (bf16[352,256]{1,0:T(8,128)(2,1)S(1)}, bf16[352,256]{1,0:T(8,128)(2,1)}, u32[]{:S(2)}) copy-start(bf16[352,256]{1,0:T(8,128)(2,1)} %param.9) | copy-start | bytes 540676
  7.2 43.4 %all-gather.6.cloned.1.call-start = ((), (), s32[]{:S(2)}) async-start(), calls=%async_computation.4 | async-start | bytes 1769472 | tf_op jit(solution)/shard_map/all_gather | solution.py:53
  7.9 54.9 %all-gather.4.cloned.1.call-start = ((), (), s32[]{:S(2)}) async-start(), calls=%async_computation.3 | async-start | bytes 1769472 | tf_op jit(solution)/shard_map/all_gather | solution.py:54
  8.7 92.7 %reduce-scatter.8.cloned.1.call-start = ((), (), s32[]{:S(2)}) async-start(), calls=%async_computation.6 | async-start | bytes 2703360 | tf_op jit(solution)/shard_map/reduce_scatter | solution.py:9
  50.6 2.3 %copy-start.2 = (bf16[768,1024]{1,0:T(8,128)(2,1)S(1)}, bf16[768,1024]{1,0:T(8,128)(2,1)}, u32[]{:S(2)}) copy-start(bf16[768,1024]{1,0:T(8,128)(2,1)} %all-gather.6.cloned.1.call-done) | copy-start | bytes 4718596
  62.8 2.3 %copy-start.4 = (bf16[768,1024]{1,0:T(8,128)(2,1)S(1)}, bf16[768,1024]{1,0:T(8,128)(2,1)}, u32[]{:S(2)}) copy-start(bf16[768,1024]{1,0:T(8,128)(2,1)} %all-gather.4.cloned.1.call-done) | copy-start | bytes 4718596
  62.8 2.3 %copy-start.5 = (bf16[768,352]{0,1:T(8,128)(2,1)S(1)}, bf16[768,352]{0,1:T(8,128)(2,1)}, u32[]{:S(2)}) copy-start(bf16[768,352]{0,1:T(8,128)(2,1)} %convolution_convert_fusion.1) | copy-start | bytes 1622020
  65.2 2.6 %copy-start.7 = (bf16[768,352]{0,1:T(8,128)(2,1)}, bf16[768,352]{0,1:T(8,128)(2,1)S(1)}, u32[]{:S(2)}) copy-start(bf16[768,352]{0,1:T(8,128)(2,1)S(1)} %convolution_convert_fusion.2) | copy-start | bytes 1622020
  65.2 1.6 copy-start.3
  70.7 32.8 %copy-start.6 = (bf16[768,352]{0,1:T(8,128)(2,1)S(1)}, bf16[768,352]{0,1:T(8,128)(2,1)}, u32[]{:S(2)}) copy-start(bf16[768,352]{0,1:T(8,128)(2,1)} %convolution_convert_fusion.1) | copy-start | bytes 1622020
  70.7 32.8 %copy-start.8 = (bf16[768,352]{0,1:T(8,128)(2,1)S(1)}, bf16[768,352]{0,1:T(8,128)(2,1)}, u32[]{:S(2)}) copy-start(bf16[768,352]{0,1:T(8,128)(2,1)} %copy-done.7) | copy-start | bytes 1622020
  70.7 54.8 %reduce-scatter.10.cloned.1.call-start = ((), (), s32[]{:S(2)}) async-start(), calls=%async_computation.7 | async-start | bytes 737280 | tf_op jit(solution)/shard_map/reduce_scatter | solution.py:20
  103.5 57.4 %reduce-scatter.6.cloned.1.call-start = ((), (), s32[]{:S(2)}) async-start(), calls=%async_computation.5 | async-start | bytes 1769472 | tf_op jit(solution)/shard_map/reduce_scatter | solution.py:9
Sparse Core Ops, SparseCore 0:
  9.7 26.8 all-gather.5
  38.2 24.5 all-gather.3
  70.8 30.4 reduce-scatter.7
  103.6 21.8 reduce-scatter.9
  128.3 32.5 reduce-scatter.5
where the time goes:
time: 168 us; the launch traced here: 167 us
  waiting for transfers between devices  77.9 us (46%)
  blocking collectives  55 us (33%)
  between operations  13.9 us (8%)
  matrix products  12.5 us (7%)
  local copies, waits for them, and re-layouts  5.9 us (4%)
  other arithmetic  2.08 us (1%)
    reduce_scatter x2, waiting for transfers between devices, summed_rows(): lax.psum_scatter(everything.astype(jnp.bfloat16), axis, scatter_dimension...  49.8 us
    reduce_scatter x1, waiting for transfers between devices, total_of(): lax.psum_scatter(padded_to(lines, lax.axis_size(axis)), axis, scatter_dim...  18.3 us
    all_gather x1, blocking collectives, body(): lax.all_gather(down_weight, 'fs', axis=1, tiled=True)  14.3 us
    all_gather x1, blocking collectives, body(): lax.all_gather(gate_weight, 'fs', axis=0, tiled=True)  14.1 us
    all_gather x1, blocking collectives, body(): lax.all_gather(up_weight, 'fs', axis=0, tiled=True)  13.5 us
    all_gather x1, blocking collectives, total_of(): whole = lax.all_gather(own, axis).reshape(-1, *lines.shape[1:])  13.1 us
    all_gather x1, waiting for transfers between devices, body(): lax.all_gather(out_grad, 'tp', axis=0, tiled=True)  8.36 us
    dot_general x3, matrix products, contract_last(): lax.dot_general(left, right, (((1,), (1,)), ((), ())), preferred_element_...  5.94 us
  transfers between devices with their start and end apart: 5, of which 4 were waited for; matrix products, arithmetic and copies ran while one was open for 6% of the time, Pallas kernels for 0%

commit v1 on v0

v1 whole, which is shorter than its diff:
```python
import functools

import jax
import jax.numpy as jnp
from jax import lax
from jax.experimental import pallas as pl
from jax.experimental.pallas import tpu as pltpu
from jax.sharding import PartitionSpec as P

MESH = pl.DeviceIdType.MESH
F32 = jnp.float32
BF16 = jnp.bfloat16

ROWS = 96
WIDTH = 1024
HID = 352
SHARD = 256
TOK = 768
R1 = 640
R2 = 448
RP = R1 + R2
Q1, Q2 = R1 // 4, R2 // 4


def nt(a, b):
    return lax.dot_general(a, b, (((1,), (1,)), ((), ())), preferred_element_type=F32)


def nn(a, b):
    return lax.dot_general(a, b, (((1,), (0,)), ((), ())), preferred_element_type=F32)


def aligned(value, by):
    return pl.multiple_of(value, by)


def kernel(factor, x_hbm, o_hbm, g_hbm, u_hbm, d_hbm, gi_ref, og_ref, ou_ref, od_ref,
           xa, oa, w, fwd, l, lt, p, out, pb, rb, s0, sb, xr, xs,
           ya, ys, yr, za, zs, zb0, zb1, zc0, zc1, zr, yb0, yb1, yc0, yc1,
           ls, ss, rs):
    z = lax.axis_index("rep")
    y = lax.axis_index("fs")
    t = lax.axis_index("tp")
    core = lax.rem(t, 2)
    half = lax.rem(z, 2)
    xp = (z, y, lax.rem(t + 2, 8))
    xm = (z, y, lax.rem(t + 6, 8))
    twin = (z, y, t + 1 - 2 * core)
    yp = (z, lax.rem(y + 1, 4), t)
    ym = (z, lax.rem(y + 3, 4), t)
    zp = (lax.rem(z + 1, 4), y, t)
    zm = (lax.rem(z + 3, 4), y, t)

    counter = [0]
    started = []

    def send(src, dst, dev):
        i = counter[0]
        counter[0] += 1
        copy = pltpu.make_async_remote_copy(
            src_ref=src, dst_ref=dst, send_sem=ss.at[i], recv_sem=rs.at[i],
            device_id=dev, device_id_type=MESH)
        copy.start()
        started.append(copy)
        return copy

    mine = pl.ds(aligned(y * SHARD, SHARD), SHARD)
    locals_ = [
        pltpu.make_async_copy(x_hbm, xa.at[pl.ds(0, ROWS)], ls.at[0]),
        pltpu.make_async_copy(g_hbm, w.at[pl.ds(0, HID), mine], ls.at[1]),
        pltpu.make_async_copy(u_hbm, w.at[pl.ds(HID, HID), mine], ls.at[2]),
        pltpu.make_async_copy(d_hbm, w.at[pl.ds(2 * HID, HID), mine], ls.at[3]),
        pltpu.make_async_copy(o_hbm, oa.at[pl.ds(0, ROWS)], ls.at[4]),
    ]
    for c in locals_:
        c.start()

    barrier = pltpu.get_barrier_semaphore()
    for dev in (xp, xm, twin, yp, ym, zp, zm):
        pl.semaphore_signal(barrier, inc=1, device_id=dev, device_id_type=MESH)
    l[pl.ds(3 * HID, RP - 3 * HID), :] = jnp.zeros((RP - 3 * HID, TOK), BF16)
    pl.semaphore_wait(barrier, 7)

    def slot(k, rel):
        return 384 * rel + ROWS * k

    def tok(ref, row, n):
        return ref.at[pl.ds(row, n)]

    my_rows = [aligned(640 * half, 16), aligned(640 * half + 208, 16), 416]

    def wblk(row, n, col):
        return w.at[pl.ds(row, n), pl.ds(aligned(lax.rem(col, 4) * SHARD, SHARD), SHARD)]

    def wsend(i, off, n, col, dev):
        ref = wblk(my_rows[i] + off if off else my_rows[i], n, col)
        return send(ref, ref, dev)

    for c in locals_[:1]:
        c.wait()
    x_p = send(tok(xa, 0, ROWS), tok(xa, slot(1, 0), ROWS), xp)
    x_m = send(tok(xa, 0, ROWS), tok(xa, slot(2, 0), ROWS), xm)
    x_t = send(tok(xa, 0, ROWS), tok(xa, slot(0, 1), ROWS), twin)
    for c in locals_[1:4]:
        c.wait()
    wp_a = wsend(0, 0, 208, y, yp)
    wm_b = wsend(1, 0, 208, y, ym)
    wp_b = wsend(1, 0, 208, y, yp)
    wm_a = wsend(0, 0, 208, y, ym)
    locals_[4].wait()
    o_p = send(tok(oa, 0, ROWS), tok(oa, slot(1, 0), ROWS), xp)
    o_m = send(tok(oa, 0, ROWS), tok(oa, slot(2, 0), ROWS), xm)
    o_t = send(tok(oa, 0, ROWS), tok(oa, slot(0, 1), ROWS), twin)

    z_in = []

    def zsend(i, col, dev):
        z_in.append(wsend(i, 0, 208, col, dev))

    wp_a.wait_recv()
    fp_a = wsend(0, 0, 208, y + 3, yp)
    zsend(0, y + 3, zp)
    wm_b.wait_recv()
    fm_b = wsend(1, 0, 208, y + 1, ym)
    zsend(1, y + 1, zm)
    wp_c = wsend(2, 0, 224, y, yp)
    wm_c = wsend(2, 0, 224, y, ym)

    x_p.wait_recv()
    xf_p = send(tok(xa, slot(1, 0), 48), tok(xa, slot(3, 0), 48), xp)
    x_m.wait_recv()
    xf_m = send(tok(xa, slot(2, 0) + 48, 48), tok(xa, slot(3, 0) + 48, 48), xm)
    xt1 = send(tok(xa, slot(1, 0), ROWS), tok(xa, slot(1, 1), ROWS), twin)
    xt2 = send(tok(xa, slot(2, 0), ROWS), tok(xa, slot(2, 1), ROWS), twin)

    wp_b.wait_recv()
    zsend(1, y + 3, zm)
    wm_a.wait_recv()
    zsend(0, y + 1, zp)
    fp_a.wait_recv()
    zsend(0, y + 2, zp)
    fm_b.wait_recv()
    zsend(1, y + 2, zm)

    o_p.wait_recv()
    of_p = send(tok(oa, slot(1, 0), 48), tok(oa, slot(3, 0), 48), xp)
    o_m.wait_recv()
    of_m = send(tok(oa, slot(2, 0) + 48, 48), tok(oa, slot(3, 0) + 48, 48), xm)
    ot1 = send(tok(oa, slot(1, 0), ROWS), tok(oa, slot(1, 1), ROWS), twin)
    ot2 = send(tok(oa, slot(2, 0), ROWS), tok(oa, slot(2, 1), ROWS), twin)

    wp_c.wait_recv()
    fp_c = wsend(2, 0, 112, y + 3, yp)
    wm_c.wait_recv()
    fm_c = wsend(2, 112, 112, y + 1, ym)

    xf_p.wait_recv()
    xf_m.wait_recv()
    xt3 = send(tok(xa, slot(3, 0), ROWS), tok(xa, slot(3, 1), ROWS), twin)
    of_p.wait_recv()
    of_m.wait_recv()
    ot3 = send(tok(oa, slot(3, 0), ROWS), tok(oa, slot(3, 1), ROWS), twin)

    for c in (fp_c, fm_c):
        c.wait_recv()
    for c in z_in:
        c.wait_recv()
    for c in (x_t, o_t, xt1, xt2, ot1, ot2, xt3, ot3):
        c.wait_recv()

    for n in range(3):
        cols = pl.ds(256 * n, 256)
        fwd[0:704, :] = nt(w[0:704, :], xa[cols, :])
        fwd[704:1056, :] = nt(w[704:1056, :], oa[cols, :])
        for m in range(11):
            a = 32 * m
            g = fwd[a:a + 32, :].astype(BF16).astype(F32)
            u = fwd[HID + a:HID + a + 32, :].astype(BF16).astype(F32)
            gh = fwd[2 * HID + a:2 * HID + a + 32, :].astype(BF16).astype(F32)
            sig = 1.0 / (1.0 + jnp.exp(-g))
            act = g * sig
            l[a:a + 32, cols] = (gh * u * sig * (1.0 + g * (1.0 - sig))).astype(BF16)
            l[HID + a:HID + a + 32, cols] = (gh * act).astype(BF16)
            l[2 * HID + a:2 * HID + a + 32, cols] = (act * u).astype(BF16)

    def shard_cols(r):
        return pl.ds(aligned(lax.rem(y + r, 4) * SHARD, SHARD), SHARD)

    def first_part(r):
        p[r, 0:R1, :] = nn(l[0:R1, :], xa[:, shard_cols(r)]).astype(BF16)

    def second_part(r):
        p[r, R1:704, :] = nn(l[R1:704, :], xa[:, shard_cols(r)]).astype(BF16)
        p[r, 704:RP, :] = nn(l[704:RP, :], oa[:, shard_cols(r)]).astype(BF16)

    class Ring:
        def __init__(self, block, load, b0, b1, c0, c1, plus, minus):
            self.block, self.load = block, load
            self.b0, self.b1, self.c0, self.c1 = b0, b1, c0, c1
            self.plus, self.minus = plus, minus

        def far(self):
            self.a0 = send(self.block(2, 0), self.b0.at[0], self.plus)
            self.a1 = send(self.block(2, 1), self.b1.at[0], self.minus)

        def near(self):
            self.n1 = send(self.block(1, 1), self.b1.at[1], self.plus)
            self.n0 = send(self.block(3, 0), self.b0.at[1], self.minus)

        def middle(self):
            self.a0.wait_recv()
            self.c0[...] = (self.b0[0].astype(F32) + self.load(1, 0).astype(F32)).astype(BF16)
            self.e0 = send(self.c0, self.b0.at[2], self.plus)
            self.a1.wait_recv()
            self.c1[...] = (self.b1[0].astype(F32) + self.load(3, 1).astype(F32)).astype(BF16)
            self.e1 = send(self.c1, self.b1.at[2], self.minus)

        def end(self):
            for c in (self.n0, self.e0, self.n1, self.e1):
                c.wait_recv()
            h0 = self.load(0, 0).astype(F32) + self.b0[1].astype(F32) + self.b0[2].astype(F32)
            h1 = self.load(0, 1).astype(F32) + self.b1[1].astype(F32) + self.b1[2].astype(F32)
            return h0, h1

    class Spread:
        def __init__(self, base, size, cut):
            self.base, self.size, self.cut = base, size, cut

        def rows(self, r, off, n):
            return out.at[pl.ds(aligned(self.base + self.size * lax.rem(z + r, 4) + off, 16), n)]

        def start(self):
            ref = self.rows(0, 0, self.size)
            self.s0 = send(ref, ref, zp)
            self.s1 = send(ref, ref, zm)

        def middle(self):
            self.s0.wait_recv()
            ref = self.rows(3, 0, self.cut)
            self.f0 = send(ref, ref, zp)
            self.s1.wait_recv()
            ref = self.rows(1, self.cut, self.size - self.cut)
            self.f1 = send(ref, ref, zm)

        def end(self):
            self.f0.wait_recv()
            self.f1.wait_recv()

    def p1(r, h):
        return p.at[r, pl.ds(320 * h, 320)]

    y_first = Ring(p1, lambda r, h: p[r, 320 * h:320 * h + 320, :],
                   ya.at[0], ya.at[1], ys.at[0], ys.at[1], yp, ym)

    def q1(r, h):
        return pl.ds(aligned(Q1 * lax.rem(z + r, 4) + 80 * h, 16), 80)

    y_then = Ring(lambda r, h: yr.at[q1(r, h)], lambda r, h: yr[q1(r, h), :],
                  za.at[0], za.at[1], zs.at[0], zs.at[1], zp, zm)
    y_out = Spread(0, Q1, 80)

    def q2(r, h):
        return pl.ds(aligned(R1 + Q2 * lax.rem(z + r, 4) + 64 * h, 16), 48 if h else 64)

    z_first = Ring(lambda r, h: p.at[:, q2(r, h)], lambda r, h: p[:, q2(r, h), :],
                   zb0, zb1, zc0, zc1, zp, zm)
    def zh(h):
        return pl.ds(64 * h, 48 if h else 64)
    z_then = Ring(lambda r, h: zr.at[r, zh(h)], lambda r, h: zr[r, zh(h), :],
                  yb0, yb1, yc0, yc1, yp, ym)
    z_out = Spread(R1, Q2, 64)

    first_part(2)
    y_first.far()
    for r in (2, 1, 3, 0):
        second_part(r)
    z_first.far()
    z_first.near()
    first_part(1)
    first_part(3)
    y_first.near()

    lt[...] = l[0:704, :].T
    for n in range(4):
        cols = pl.ds(256 * n, 256)
        pb[:, cols] = nn(lt[384:768, :], w[0:704, cols]).astype(BF16)
    pair = send(pb, rb, twin)
    for n in range(4):
        cols = pl.ds(256 * n, 256)
        s0[:, cols] = nn(lt[0:384, :], w[0:704, cols])

    y_first.middle()
    z_first.middle()
    pair.wait_recv()
    sb[...] = (s0[...] + rb[...].astype(F32)).astype(BF16)
    chip = {0: 0, 3: 1, 1: 2, 2: 3}
    def xh(r, h):
        return pl.ds(ROWS * chip[r] + 48 * h, 48)
    x_ring = Ring(lambda r, h: sb.at[xh(r, h)], lambda r, h: sb[xh(r, h), :],
                  xr.at[0], xr.at[1], xs.at[0], xs.at[1], xp, xm)
    x_ring.far()
    x_ring.near()
    first_part(0)

    h0, h1 = z_first.end()
    zr[:, 0:64, :] = h0.astype(BF16)
    zr[:, 64:112, :] = h1.astype(BF16)
    z_then.far()
    z_then.near()
    h0, h1 = y_first.end()
    yr[0:320, :] = h0.astype(BF16)
    yr[320:640, :] = h1.astype(BF16)
    y_then.far()
    y_then.near()
    x_ring.middle()
    z_then.middle()
    y_then.middle()
    h0, h1 = z_then.end()
    out[z_out_rows(z, 0), :] = h0.astype(BF16)
    out[z_out_rows(z, 1), :] = h1.astype(BF16)
    z_out.start()
    h0, h1 = y_then.end()
    out[q1(0, 0), :] = h0.astype(BF16)
    out[q1(0, 1), :] = h1.astype(BF16)
    y_out.start()
    h0, h1 = x_ring.end()
    gi_ref[0:48, :] = h0.astype(BF16)
    gi_ref[48:96, :] = h1.astype(BF16)
    z_out.middle()
    y_out.middle()
    z_out.end()
    y_out.end()
    og_ref[...] = out[0:HID, :].astype(F32) * factor
    ou_ref[...] = out[HID:2 * HID, :].astype(F32) * factor
    od_ref[...] = out[2 * HID:3 * HID, :].astype(F32) * factor
    for c in started:
        c.wait_send()


def z_out_rows(z, h):
    return pl.ds(pl.multiple_of(R1 + Q2 * z + 64 * h, 16), 48 if h else 64)


def body(tokens_in, out_grad, gate_weight, up_weight, down_weight):
    factor = (ROWS * 128) ** (-0.5)
    vmem = pl.BlockSpec(memory_space=pltpu.VMEM)
    grad_in, gg, gu, gd = pl.pallas_call(
        functools.partial(kernel, factor),
        name="ffn_backward",
        out_shape=(
            jax.ShapeDtypeStruct((ROWS, WIDTH), BF16),
            jax.ShapeDtypeStruct((HID, SHARD), F32),
            jax.ShapeDtypeStruct((HID, SHARD), F32),
            jax.ShapeDtypeStruct((HID, SHARD), F32),
        ),
        in_specs=[pl.BlockSpec(memory_space=pl.ANY)] * 5,
        out_specs=(vmem,) * 4,
        scratch_shapes=[
            pltpu.VMEM((TOK, WIDTH), BF16),
            pltpu.VMEM((TOK, WIDTH), BF16),
            pltpu.VMEM((3 * HID, WIDTH), BF16),
            pltpu.VMEM((3 * HID, 256), F32),
            pltpu.VMEM((RP, TOK), BF16),
            pltpu.VMEM((TOK, 2 * HID), BF16),
            pltpu.VMEM((4, RP, SHARD), BF16),
            pltpu.VMEM((RP, SHARD), BF16),
            pltpu.VMEM((384, WIDTH), BF16),
            pltpu.VMEM((384, WIDTH), BF16),
            pltpu.VMEM((384, WIDTH), F32),
            pltpu.VMEM((384, WIDTH), BF16),
            pltpu.VMEM((2, 3, 48, WIDTH), BF16),
            pltpu.VMEM((2, 48, WIDTH), BF16),
            pltpu.VMEM((2, 3, 320, SHARD), BF16),
            pltpu.VMEM((2, 320, SHARD), BF16),
            pltpu.VMEM((R1, SHARD), BF16),
            pltpu.VMEM((2, 3, 80, SHARD), BF16),
            pltpu.VMEM((2, 80, SHARD), BF16),
            pltpu.VMEM((3, 4, 64, SHARD), BF16),
            pltpu.VMEM((3, 4, 48, SHARD), BF16),
            pltpu.VMEM((4, 64, SHARD), BF16),
            pltpu.VMEM((4, 48, SHARD), BF16),
            pltpu.VMEM((4, Q2, SHARD), BF16),
            pltpu.VMEM((3, 64, SHARD), BF16),
            pltpu.VMEM((3, 48, SHARD), BF16),
            pltpu.VMEM((64, SHARD), BF16),
            pltpu.VMEM((48, SHARD), BF16),
            pltpu.SemaphoreType.DMA((5,)),
            pltpu.SemaphoreType.DMA((80,)),
            pltpu.SemaphoreType.DMA((80,)),
        ],
        compiler_params=pltpu.CompilerParams(collective_id=0, has_side_effects=True),
    )(tokens_in, out_grad, gate_weight.T, up_weight.T, down_weight)
    return grad_in, gg.T, gu.T, gd


def solution(mesh):
    return jax.shard_map(
        body,
        mesh=mesh,
        in_specs=(
            P(("rep", "fs", "tp"), None),
            P(("rep", "fs", "tp"), None),
            P("fs", "tp"),
            P("fs", "tp"),
            P("tp", "fs"),
        ),
        out_specs=(P(("rep", "fs", "tp"), None), P("fs", "tp"), P("fs", "tp"), P("tp", "fs")),
        check_vma=False,
    )
```

time: 168 us -> 60.6 us (0.36)
  waiting for transfers between devices: 77.9 us -> 0 us
  Pallas kernels: 0 us -> 55.1 us
  blocking collectives: 55 us -> 0 us
  between operations: 13.9 us -> 0.65 us
  matrix products: 12.5 us -> 0 us
  other arithmetic: 2.08 us -> 0 us
    reduce_scatter x3 -> x0, waiting for transfers between devices: 68.1 us -> none  [the longest x2 49.8 us: summed_rows(): lax.psum_scatter(everything.astype(jnp.bfloat16), axis, scatter_dimension...]
    pallas_call x0 -> x1, Pallas kernels: none -> 55.1 us  [body(): pl.pallas_call(functools.partial(kernel, factor), name='ffn_backward', ou...]
    all_gather x4 -> x0, blocking collectives: 55 us -> none  [the longest x1 14.3 us: body(): lax.all_gather(down_weight, 'fs', axis=1, tiled=True)]
    dot_general x8 -> x0, matrix products: 12.5 us -> none  [the longest x3 5.94 us: contract_last(): lax.dot_general(left, right, (((1,), (1,)), ((), ())), preferred_element_...]
    all_gather x2 -> x0, waiting for transfers between devices: 8.37 us -> none  [the longest x1 8.36 us: body(): lax.all_gather(out_grad, 'tp', axis=0, tiled=True)]
    convert_element_type x2 -> x0, other arithmetic: 2.08 us -> none  [the longest x1 2.01 us: summed_rows(): everything.astype(jnp.bfloat16)]
    unnamed x22 -> x10, local copies, waits for them, and re-layouts: 5.62 us -> 4.63 us
  transfers between devices with their start and end apart: 5 -> 0, of which waited for: 4 -> 0; matrix products, arithmetic and copies ran while one was open for 6% -> 0% of each run, Pallas kernels for 0% -> 0%
where the time goes in v1:
time: 60.6 us; the launch traced here: 60.4 us
  Pallas kernels  55.1 us (91%)
  local copies, waits for them, and re-layouts  4.63 us (8%)
  between operations  0.65 us (1%)
    pallas_call x1, Pallas kernels, body(): pl.pallas_call(functools.partial(kernel, factor), name='ffn_backward', ou...  55.1 us
    unnamed x10, local copies, waits for them, and re-layouts  4.63 us

profile of v1, /device:TPU:0, one launch (start us, length us, event | category | flops | bytes accessed | tf_op | source)
XLA Modules:
  0.0 60.4 jit_solution(3118973604786107939)
XLA Ops:
  0.6 55.1 %ffn_backward.1 = (bf16[96,1024]{1,0:T(8,128)(2,1)}, f32[352,256]{1,0:T(8,128)}, f32[352,256]{1,0:T(8,128)}, f32[352,256]{1,0:T(8,128)}) custom-call(bf16[96,1024]{1,0:T(8,128)(2,1)} %x_hbm.1, bf16[96,1024]{1,0:T(8,128)(2,1)} %o_hbm.1, bf16[352,256]{1,0:T(8,128)(2,1)} %bitcast.6, bf16[352,256]{1,0:T(8,128)(2,1)} %bitcast.7, bf16[352,256]{1,0:T(8,128)(2,1)} %d_hbm.1), custom_call_target="tpu_custom_call" | custom-call | tf_op jit(solution)/shard_map/ffn_backward/pallas_call | solution.py:347
  55.7 0.0 copy-start.2
  55.7 1.7 %copy.13 = bf16[96,1024]{1,0:T(8,128)(2,1)} copy(bf16[96,1024]{1,0:T(8,128)(2,1)} %get-tuple-element.16) | data formatting | bytes 393216
  57.4 0.0 copy-done.2
  57.4 0.0 copy-start.1
  57.4 0.7 %copy.14 = f32[256,352]{0,1:T(8,128)} copy(f32[256,352]{0,1:T(8,128)S(1)} %bitcast.5) | data formatting | bytes 720896
  58.1 0.4 copy-done.1
  58.5 0.0 copy-start
  58.5 0.7 %copy.15 = f32[256,352]{0,1:T(8,128)} copy(f32[256,352]{0,1:T(8,128)S(1)} %bitcast.4) | data formatting | bytes 720896
  59.3 0.4 copy-done
  59.6 0.7 %copy.16 = f32[352,256]{1,0:T(8,128)} copy(f32[352,256]{1,0:T(8,128)S(1)} %copy-done) | data formatting | bytes 720896
Async XLA Ops:
  55.7 1.7 %copy-start.2 = (f32[352,256]{1,0:T(8,128)S(1)}, f32[352,256]{1,0:T(8,128)}, u32[]{:S(2)}) copy-start(f32[352,256]{1,0:T(8,128)} %get-tuple-element.9) | copy-start | bytes 1081348
  57.4 1.1 %copy-start.1 = (f32[352,256]{1,0:T(8,128)S(1)}, f32[352,256]{1,0:T(8,128)}, u32[]{:S(2)}) copy-start(f32[352,256]{1,0:T(8,128)} %get-tuple-element.10) | copy-start | bytes 1081348
  58.5 1.1 %copy-start = (f32[352,256]{1,0:T(8,128)S(1)}, f32[352,256]{1,0:T(8,128)}, u32[]{:S(2)}) copy-start(f32[352,256]{1,0:T(8,128)} %get-tuple-element.19) | copy-start | bytes 1081348

commit v2 on v1

--- a/solution.py
+++ b/solution.py
@@ -16,8 +16,9 @@
 HID = 352
 SHARD = 256
 TOK = 768
-R1 = 640
-R2 = 448
+EARLY = 512
+R1 = 576
+R2 = 512
 RP = R1 + R2
 Q1, Q2 = R1 // 4, R2 // 4
 
@@ -34,9 +35,9 @@
     return pl.multiple_of(value, by)
 
 
-def kernel(factor, x_hbm, o_hbm, g_hbm, u_hbm, d_hbm, gi_ref, og_ref, ou_ref, od_ref,
-           xa, oa, w, fwd, l, lt, p, out, pb, rb, s0, sb, xr, xs,
-           ya, ys, yr, za, zs, zb0, zb1, zc0, zc1, zr, yb0, yb1, yc0, yc1,
+def kernel(x_hbm, o_hbm, g_hbm, u_hbm, d_hbm, gi_ref, dw_ref,
+           xa, oa, w, fwd, l, lt, pa, p, out, pb, rb, s0, sb, xr, xs,
+           ya, ys, yr, za0, za1, zs0, zs1, zb0, zb1, zc0, zc1, zr, yb0, yb1, yc0, yc1,
            ls, ss, rs):
     z = lax.axis_index("rep")
     y = lax.axis_index("fs")
@@ -82,7 +83,7 @@
     pl.semaphore_wait(barrier, 7)
 
     def slot(k, rel):
-        return 384 * rel + ROWS * k
+        return 2 * ROWS * k + ROWS * rel
 
     def tok(ref, row, n):
         return ref.at[pl.ds(row, n)]
@@ -142,6 +143,11 @@
     fm_b.wait_recv()
     zsend(1, y + 2, zm)
 
+    wp_c.wait_recv()
+    fp_c = wsend(2, 0, 112, y + 3, yp)
+    wm_c.wait_recv()
+    fm_c = wsend(2, 112, 112, y + 1, ym)
+
     o_p.wait_recv()
     of_p = send(tok(oa, slot(1, 0), 48), tok(oa, slot(3, 0), 48), xp)
     o_m.wait_recv()
@@ -149,34 +155,22 @@
     ot1 = send(tok(oa, slot(1, 0), ROWS), tok(oa, slot(1, 1), ROWS), twin)
     ot2 = send(tok(oa, slot(2, 0), ROWS), tok(oa, slot(2, 1), ROWS), twin)
 
-    wp_c.wait_recv()
-    fp_c = wsend(2, 0, 112, y + 3, yp)
-    wm_c.wait_recv()
-    fm_c = wsend(2, 112, 112, y + 1, ym)
-
-    xf_p.wait_recv()
-    xf_m.wait_recv()
-    xt3 = send(tok(xa, slot(3, 0), ROWS), tok(xa, slot(3, 1), ROWS), twin)
-    of_p.wait_recv()
-    of_m.wait_recv()
-    ot3 = send(tok(oa, slot(3, 0), ROWS), tok(oa, slot(3, 1), ROWS), twin)
-
     for c in (fp_c, fm_c):
         c.wait_recv()
     for c in z_in:
         c.wait_recv()
-    for c in (x_t, o_t, xt1, xt2, ot1, ot2, xt3, ot3):
+    for c in (x_t, o_t, xt1, xt2, ot1, ot2):
         c.wait_recv()
 
-    for n in range(3):
-        cols = pl.ds(256 * n, 256)
-        fwd[0:704, :] = nt(w[0:704, :], xa[cols, :])
-        fwd[704:1056, :] = nt(w[704:1056, :], oa[cols, :])
+    def forward(c0, n):
+        cols = pl.ds(c0, n)
+        for part, source in ((0, xa), (HID, xa), (2 * HID, oa)):
+            fwd[part:part + HID, 0:n] = nt(w[part:part + HID, :], source[cols, :])
         for m in range(11):
             a = 32 * m
-            g = fwd[a:a + 32, :].astype(BF16).astype(F32)
-            u = fwd[HID + a:HID + a + 32, :].astype(BF16).astype(F32)
-            gh = fwd[2 * HID + a:2 * HID + a + 32, :].astype(BF16).astype(F32)
+            g = fwd[a:a + 32, 0:n].astype(BF16).astype(F32)
+            u = fwd[HID + a:HID + a + 32, 0:n].astype(BF16).astype(F32)
+            gh = fwd[2 * HID + a:2 * HID + a + 32, 0:n].astype(BF16).astype(F32)
             sig = 1.0 / (1.0 + jnp.exp(-g))
             act = g * sig
             l[a:a + 32, cols] = (gh * u * sig * (1.0 + g * (1.0 - sig))).astype(BF16)
@@ -186,12 +180,39 @@
     def shard_cols(r):
         return pl.ds(aligned(lax.rem(y + r, 4) * SHARD, SHARD), SHARD)
 
+    def early(r):
+        pa[r, 0:704, :] = nn(l[0:704, 0:EARLY], xa[0:EARLY, shard_cols(r)])
+        pa[r, 704:RP, :] = nn(l[704:RP, 0:EARLY], oa[0:EARLY, shard_cols(r)])
+
+    def late(r, row, n, source):
+        rows = pl.ds(row, n)
+        p[r, rows, :] = (pa[r, rows, :] + nn(l[rows, EARLY:TOK], source[EARLY:TOK, shard_cols(r)])).astype(BF16)
+
     def first_part(r):
-        p[r, 0:R1, :] = nn(l[0:R1, :], xa[:, shard_cols(r)]).astype(BF16)
+        late(r, 0, R1 // 2, xa)
+        late(r, R1 // 2, R1 // 2, xa)
 
     def second_part(r):
-        p[r, R1:704, :] = nn(l[R1:704, :], xa[:, shard_cols(r)]).astype(BF16)
-        p[r, 704:RP, :] = nn(l[704:RP, :], oa[:, shard_cols(r)]).astype(BF16)
+        late(r, R1, 704 - R1, xa)
+        late(r, 704, RP - 704, oa)
+
+    forward(0, EARLY)
+    xf_p.wait_recv()
+    xt3 = send(tok(xa, slot(3, 0), 48), tok(xa, slot(3, 1), 48), twin)
+    xf_m.wait_recv()
+    xt4 = send(tok(xa, slot(3, 0) + 48, 48), tok(xa, slot(3, 1) + 48, 48), twin)
+    for r in (2, 1):
+        early(r)
+    of_p.wait_recv()
+    ot3 = send(tok(oa, slot(3, 0), 48), tok(oa, slot(3, 1), 48), twin)
+    for r in (3, 0):
+        early(r)
+    of_m.wait_recv()
+    ot4 = send(tok(oa, slot(3, 0) + 48, 48), tok(oa, slot(3, 1) + 48, 48), twin)
+    lt[0:EARLY, :] = l[0:704, 0:EARLY].T
+    for c in (xt3, xt4, ot3, ot4):
+        c.wait_recv()
+    forward(EARLY, TOK - EARLY)
 
     class Ring:
         def __init__(self, block, load, b0, b1, c0, c1, plus, minus):
@@ -247,25 +268,25 @@
             self.f1.wait_recv()
 
     def p1(r, h):
-        return p.at[r, pl.ds(320 * h, 320)]
-
-    y_first = Ring(p1, lambda r, h: p[r, 320 * h:320 * h + 320, :],
+        return p.at[r, pl.ds(R1 // 2 * h, R1 // 2)]
+
+    y_first = Ring(p1, lambda r, h: p[r, R1 // 2 * h:R1 // 2 * (h + 1), :],
                    ya.at[0], ya.at[1], ys.at[0], ys.at[1], yp, ym)
 
     def q1(r, h):
-        return pl.ds(aligned(Q1 * lax.rem(z + r, 4) + 80 * h, 16), 80)
+        return pl.ds(aligned(Q1 * lax.rem(z + r, 4) + 80 * h, 16), 64 if h else 80)
 
     y_then = Ring(lambda r, h: yr.at[q1(r, h)], lambda r, h: yr[q1(r, h), :],
-                  za.at[0], za.at[1], zs.at[0], zs.at[1], zp, zm)
+                  za0, za1, zs0, zs1, zp, zm)
     y_out = Spread(0, Q1, 80)
 
     def q2(r, h):
-        return pl.ds(aligned(R1 + Q2 * lax.rem(z + r, 4) + 64 * h, 16), 48 if h else 64)
+        return pl.ds(aligned(R1 + Q2 * lax.rem(z + r, 4) + 64 * h, 16), 64)
 
     z_first = Ring(lambda r, h: p.at[:, q2(r, h)], lambda r, h: p[:, q2(r, h), :],
                    zb0, zb1, zc0, zc1, zp, zm)
     def zh(h):
-        return pl.ds(64 * h, 48 if h else 64)
+        return pl.ds(64 * h, 64)
     z_then = Ring(lambda r, h: zr.at[r, zh(h)], lambda r, h: zr[r, zh(h), :],
                   yb0, yb1, yc0, yc1, yp, ym)
     z_out = Spread(R1, Q2, 64)
@@ -280,14 +301,15 @@
     first_part(3)
     y_first.near()
 
-    lt[...] = l[0:704, :].T
-    for n in range(4):
-        cols = pl.ds(256 * n, 256)
-        pb[:, cols] = nn(lt[384:768, :], w[0:704, cols]).astype(BF16)
+    lt[EARLY:TOK, :] = l[0:704, EARLY:TOK].T
+
+    def token_grads(rel):
+        rows = jnp.concatenate([lt[slot(k, rel):slot(k, rel) + ROWS, :] for k in range(4)], axis=0)
+        return nn(rows, w[0:704, :])
+
+    pb[...] = token_grads(1).astype(BF16)
     pair = send(pb, rb, twin)
-    for n in range(4):
-        cols = pl.ds(256 * n, 256)
-        s0[:, cols] = nn(lt[0:384, :], w[0:704, cols])
+    s0[...] = token_grads(0)
 
     y_first.middle()
     z_first.middle()
@@ -304,12 +326,12 @@
 
     h0, h1 = z_first.end()
     zr[:, 0:64, :] = h0.astype(BF16)
-    zr[:, 64:112, :] = h1.astype(BF16)
+    zr[:, 64:128, :] = h1.astype(BF16)
     z_then.far()
     z_then.near()
     h0, h1 = y_first.end()
-    yr[0:320, :] = h0.astype(BF16)
-    yr[320:640, :] = h1.astype(BF16)
+    yr[0:R1 // 2, :] = h0.astype(BF16)
+    yr[R1 // 2:R1, :] = h1.astype(BF16)
     y_then.far()
     y_then.near()
     x_ring.middle()
@@ -330,38 +352,46 @@
     y_out.middle()
     z_out.end()
     y_out.end()
-    og_ref[...] = out[0:HID, :].astype(F32) * factor
-    ou_ref[...] = out[HID:2 * HID, :].astype(F32) * factor
-    od_ref[...] = out[2 * HID:3 * HID, :].astype(F32) * factor
+    dw_ref[...] = out[0:3 * HID, :]
     for c in started:
         c.wait_send()
 
 
 def z_out_rows(z, h):
-    return pl.ds(pl.multiple_of(R1 + Q2 * z + 64 * h, 16), 48 if h else 64)
+    return pl.ds(pl.multiple_of(R1 + Q2 * z + 64 * h, 16), 64)
+
+
+def finish(factor, gi_ref, dw_ref, gi_hbm, og_hbm, ou_hbm, od_hbm, gi, og, ou, od, sems):
+    copies = []
+    for i, (buf, dst) in enumerate(((gi, gi_hbm), (og, og_hbm), (ou, ou_hbm), (od, od_hbm))):
+        if i == 0:
+            buf[...] = gi_ref[...]
+        else:
+            buf[...] = dw_ref[HID * (i - 1):HID * i, :].astype(F32) * factor
+        copies.append(pltpu.make_async_copy(buf, dst, sems.at[i]))
+        copies[-1].start()
+    for c in copies:
+        c.wait()
 
 
 def body(tokens_in, out_grad, gate_weight, up_weight, down_weight):
     factor = (ROWS * 128) ** (-0.5)
     vmem = pl.BlockSpec(memory_space=pltpu.VMEM)
-    grad_in, gg, gu, gd = pl.pallas_call(
-        functools.partial(kernel, factor),
+    hbm = pl.BlockSpec(memory_space=pl.ANY)
+    grad_in, sums = pl.pallas_call(
+        kernel,
         name="ffn_backward",
-        out_shape=(
-            jax.ShapeDtypeStruct((ROWS, WIDTH), BF16),
-            jax.ShapeDtypeStruct((HID, SHARD), F32),
-            jax.ShapeDtypeStruct((HID, SHARD), F32),
-            jax.ShapeDtypeStruct((HID, SHARD), F32),
-        ),
+        out_shape=(pltpu.VMEM((ROWS, WIDTH), BF16), pltpu.VMEM((3 * HID, SHARD), BF16)),
         in_specs=[pl.BlockSpec(memory_space=pl.ANY)] * 5,
-        out_specs=(vmem,) * 4,
+        out_specs=(vmem, vmem),
         scratch_shapes=[
             pltpu.VMEM((TOK, WIDTH), BF16),
             pltpu.VMEM((TOK, WIDTH), BF16),
             pltpu.VMEM((3 * HID, WIDTH), BF16),
-            pltpu.VMEM((3 * HID, 256), F32),
+            pltpu.VMEM((3 * HID, EARLY), F32),
             pltpu.VMEM((RP, TOK), BF16),
             pltpu.VMEM((TOK, 2 * HID), BF16),
+            pltpu.VMEM((4, RP, SHARD), F32),
             pltpu.VMEM((4, RP, SHARD), BF16),
             pltpu.VMEM((RP, SHARD), BF16),
             pltpu.VMEM((384, WIDTH), BF16),
@@ -370,26 +400,38 @@
             pltpu.VMEM((384, WIDTH), BF16),
             pltpu.VMEM((2, 3, 48, WIDTH), BF16),
             pltpu.VMEM((2, 48, WIDTH), BF16),
-            pltpu.VMEM((2, 3, 320, SHARD), BF16),
-            pltpu.VMEM((2, 320, SHARD), BF16),
+            pltpu.VMEM((2, 3, R1 // 2, SHARD), BF16),
+            pltpu.VMEM((2, R1 // 2, SHARD), BF16),
             pltpu.VMEM((R1, SHARD), BF16),
-            pltpu.VMEM((2, 3, 80, SHARD), BF16),
-            pltpu.VMEM((2, 80, SHARD), BF16),
+            pltpu.VMEM((3, 80, SHARD), BF16),
+            pltpu.VMEM((3, 64, SHARD), BF16),
+            pltpu.VMEM((80, SHARD), BF16),
+            pltpu.VMEM((64, SHARD), BF16),
             pltpu.VMEM((3, 4, 64, SHARD), BF16),
-            pltpu.VMEM((3, 4, 48, SHARD), BF16),
+            pltpu.VMEM((3, 4, 64, SHARD), BF16),
             pltpu.VMEM((4, 64, SHARD), BF16),
-            pltpu.VMEM((4, 48, SHARD), BF16),
+            pltpu.VMEM((4, 64, SHARD), BF16),
             pltpu.VMEM((4, Q2, SHARD), BF16),
             pltpu.VMEM((3, 64, SHARD), BF16),
-            pltpu.VMEM((3, 48, SHARD), BF16),
+            pltpu.VMEM((3, 64, SHARD), BF16),
             pltpu.VMEM((64, SHARD), BF16),
-            pltpu.VMEM((48, SHARD), BF16),
+            pltpu.VMEM((64, SHARD), BF16),
             pltpu.SemaphoreType.DMA((5,)),
             pltpu.SemaphoreType.DMA((80,)),
             pltpu.SemaphoreType.DMA((80,)),
         ],
         compiler_params=pltpu.CompilerParams(collective_id=0, has_side_effects=True),
     )(tokens_in, out_grad, gate_weight.T, up_weight.T, down_weight)
+    grad_in, gg, gu, gd = pl.pallas_call(
+        functools.partial(finish, factor),
+        name="finish",
+        out_shape=(jax.ShapeDtypeStruct((ROWS, WIDTH), BF16),) + (jax.ShapeDtypeStruct((HID, SHARD), F32),) * 3,
+        in_specs=[vmem, vmem],
+        out_specs=(hbm,) * 4,
+        scratch_shapes=[pltpu.VMEM((ROWS, WIDTH), BF16)] + [pltpu.VMEM((HID, SHARD), F32)] * 3
+        + [pltpu.SemaphoreType.DMA((4,))],
+        compiler_params=pltpu.CompilerParams(vmem_limit_bytes=8 << 20),
+    )(grad_in, sums)
     return grad_in, gg.T, gu.T, gd
 
 

time: 60.6 us -> 56.1 us (0.926)
  local copies, waits for them, and re-layouts: 4.63 us -> 0 us
    unnamed x10 -> x0, local copies, waits for them, and re-layouts: 4.63 us -> none
    pallas_call x1 -> x2, Pallas kernels: 55.1 us -> 55.3 us  [the longest x1 54.2 us: body(): pl.pallas_call(kernel, name='ffn_backward', out_shape=(pltpu.VMEM((ROWS,...]
where the time goes in v2:
time: 56.1 us; the launch traced here: 56 us
  Pallas kernels  55.3 us (99%)
  between operations  0.64 us (1%)
    pallas_call x1, Pallas kernels, body(): pl.pallas_call(kernel, name='ffn_backward', out_shape=(pltpu.VMEM((ROWS,...  54.2 us

profile of v2, /device:TPU:0, one launch (start us, length us, event | category | flops | bytes accessed | tf_op | source)
XLA Modules:
  0.0 56.0 jit_solution(10273949248765376429)
XLA Ops:
  0.6 54.2 %ffn_backward.1 = (bf16[96,1024]{1,0:T(8,128)(2,1)S(1)}, bf16[1056,256]{1,0:T(8,128)(2,1)S(1)}) custom-call(bf16[96,1024]{1,0:T(8,128)(2,1)} %x_hbm.1, bf16[96,1024]{1,0:T(8,128)(2,1)} %o_hbm.1, bf16[352,256]{1,0:T(8,128)(2,1)} %bitcast.4, bf16[352,256]{1,0:T(8,128)(2,1)} %bitcast.5, bf16[352,256]{1,0:T(8,128)(2,1)} %d_hbm.1), custom_call_target="tpu_custom_call" | custom-call | tf_op jit(solution)/shard_map/ffn_backward/pallas_call | solution.py:381
  54.9 1.1 %finish.1 = (bf16[96,1024]{1,0:T(8,128)(2,1)}, f32[352,256]{1,0:T(8,128)}, f32[352,256]{1,0:T(8,128)}, f32[352,256]{1,0:T(8,128)}) custom-call(bf16[96,1024]{1,0:T(8,128)(2,1)S(1)} %get-tuple-element.10.gi_ref, bf16[1056,256]{1,0:T(8,128)(2,1)S(1)} %get-tuple-element.11.dw_ref), custom_call_target="tpu_custom_call" | custom-call | tf_op jit(solution)/shard_map/finish/pallas_call | solution.py:425

commit v3 on v2

--- a/solution.py
+++ b/solution.py
@@ -35,8 +35,8 @@
     return pl.multiple_of(value, by)
 
 
-def kernel(x_hbm, o_hbm, g_hbm, u_hbm, d_hbm, gi_ref, dw_ref,
-           xa, oa, w, fwd, l, lt, pa, p, out, pb, rb, s0, sb, xr, xs,
+def kernel(x_hbm, o_hbm, g_hbm, u_hbm, d_hbm, gi_ref, out,
+           xa, oa, w, fwd, l, lt, pa, p, pb, rb, s0, sb, xr, xs,
            ya, ys, yr, za0, za1, zs0, zs1, zb0, zb1, zc0, zc1, zr, yb0, yb1, yc0, yc1,
            ls, ss, rs):
     z = lax.axis_index("rep")
@@ -64,6 +64,10 @@
         copy.start()
         started.append(copy)
         return copy
+
+    def drain(keep=0):
+        while len(started) > keep:
+            started.pop(0).wait_send()
 
     mine = pl.ds(aligned(y * SHARD, SHARD), SHARD)
     locals_ = [
@@ -155,6 +159,10 @@
     ot1 = send(tok(oa, slot(1, 0), ROWS), tok(oa, slot(1, 1), ROWS), twin)
     ot2 = send(tok(oa, slot(2, 0), ROWS), tok(oa, slot(2, 1), ROWS), twin)
 
+    xf_p.wait_recv()
+    xt3 = send(tok(xa, slot(3, 0), 48), tok(xa, slot(3, 1), 48), twin)
+    xf_m.wait_recv()
+    xt4 = send(tok(xa, slot(3, 0) + 48, 48), tok(xa, slot(3, 1) + 48, 48), twin)
     for c in (fp_c, fm_c):
         c.wait_recv()
     for c in z_in:
@@ -180,36 +188,32 @@
     def shard_cols(r):
         return pl.ds(aligned(lax.rem(y + r, 4) * SHARD, SHARD), SHARD)
 
-    def early(r):
-        pa[r, 0:704, :] = nn(l[0:704, 0:EARLY], xa[0:EARLY, shard_cols(r)])
-        pa[r, 704:RP, :] = nn(l[704:RP, 0:EARLY], oa[0:EARLY, shard_cols(r)])
-
-    def late(r, row, n, source):
-        rows = pl.ds(row, n)
-        p[r, rows, :] = (pa[r, rows, :] + nn(l[rows, EARLY:TOK], source[EARLY:TOK, shard_cols(r)])).astype(BF16)
+    def early(row, n, source):
+        pa[row:row + n, :] = nn(l[row:row + n, 0:EARLY], source[0:EARLY, shard_cols(2)])
+
+    def late(row, n, source):
+        more = nn(l[row:row + n, EARLY:TOK], source[EARLY:TOK, shard_cols(2)])
+        p[2, row:row + n, :] = (pa[row:row + n, :] + more).astype(BF16)
+
+    def whole(r, row, n, source):
+        p[r, row:row + n, :] = nn(l[row:row + n, :], source[:, shard_cols(r)]).astype(BF16)
 
     def first_part(r):
-        late(r, 0, R1 // 2, xa)
-        late(r, R1 // 2, R1 // 2, xa)
+        whole(r, 0, R1 // 2, xa)
+        whole(r, R1 // 2, R1 // 2, xa)
 
     def second_part(r):
-        late(r, R1, 704 - R1, xa)
-        late(r, 704, RP - 704, oa)
-
-    forward(0, EARLY)
-    xf_p.wait_recv()
-    xt3 = send(tok(xa, slot(3, 0), 48), tok(xa, slot(3, 1), 48), twin)
-    xf_m.wait_recv()
-    xt4 = send(tok(xa, slot(3, 0) + 48, 48), tok(xa, slot(3, 1) + 48, 48), twin)
-    for r in (2, 1):
-        early(r)
+        whole(r, R1, 704 - R1, xa)
+        whole(r, 704, RP - 704, oa)
+
+    forward(0, 256)
     of_p.wait_recv()
     ot3 = send(tok(oa, slot(3, 0), 48), tok(oa, slot(3, 1), 48), twin)
-    for r in (3, 0):
-        early(r)
     of_m.wait_recv()
     ot4 = send(tok(oa, slot(3, 0) + 48, 48), tok(oa, slot(3, 1) + 48, 48), twin)
-    lt[0:EARLY, :] = l[0:704, 0:EARLY].T
+    forward(256, EARLY - 256)
+    early(0, R1 // 2, xa)
+    early(R1 // 2, R1 // 2, xa)
     for c in (xt3, xt4, ot3, ot4):
         c.wait_recv()
     forward(EARLY, TOK - EARLY)
@@ -221,8 +225,14 @@
             self.plus, self.minus = plus, minus
 
         def far(self):
-            self.a0 = send(self.block(2, 0), self.b0.at[0], self.plus)
-            self.a1 = send(self.block(2, 1), self.b1.at[0], self.minus)
+            self.far_half(0)
+            self.far_half(1)
+
+        def far_half(self, h):
+            if h:
+                self.a1 = send(self.block(2, 1), self.b1.at[0], self.minus)
+            else:
+                self.a0 = send(self.block(2, 0), self.b0.at[0], self.plus)
 
         def near(self):
             self.n1 = send(self.block(1, 1), self.b1.at[1], self.plus)
@@ -236,12 +246,11 @@
             self.c1[...] = (self.b1[0].astype(F32) + self.load(3, 1).astype(F32)).astype(BF16)
             self.e1 = send(self.c1, self.b1.at[2], self.minus)
 
-        def end(self):
-            for c in (self.n0, self.e0, self.n1, self.e1):
+        def end(self, h):
+            for c in ((self.n1, self.e1) if h else (self.n0, self.e0)):
                 c.wait_recv()
-            h0 = self.load(0, 0).astype(F32) + self.b0[1].astype(F32) + self.b0[2].astype(F32)
-            h1 = self.load(0, 1).astype(F32) + self.b1[1].astype(F32) + self.b1[2].astype(F32)
-            return h0, h1
+            got = self.b1 if h else self.b0
+            return (self.load(0, h).astype(F32) + got[1].astype(F32) + got[2].astype(F32)).astype(BF16)
 
     class Spread:
         def __init__(self, base, size, cut):
@@ -250,22 +259,29 @@
         def rows(self, r, off, n):
             return out.at[pl.ds(aligned(self.base + self.size * lax.rem(z + r, 4) + off, 16), n)]
 
-        def start(self):
-            ref = self.rows(0, 0, self.size)
-            self.s0 = send(ref, ref, zp)
-            self.s1 = send(ref, ref, zm)
+        def part(self, r, h):
+            return self.rows(r, self.cut * h, self.size - self.cut if h else self.cut)
+
+        def start(self, h):
+            ref = self.part(0, h)
+            if h:
+                self.m1 = send(ref, ref, zm)
+                self.p1 = send(ref, ref, zp)
+            else:
+                self.p0 = send(ref, ref, zp)
+                self.m0 = send(ref, ref, zm)
 
         def middle(self):
-            self.s0.wait_recv()
-            ref = self.rows(3, 0, self.cut)
+            self.p0.wait_recv()
+            ref = self.part(3, 0)
             self.f0 = send(ref, ref, zp)
-            self.s1.wait_recv()
-            ref = self.rows(1, self.cut, self.size - self.cut)
+            self.m1.wait_recv()
+            ref = self.part(1, 1)
             self.f1 = send(ref, ref, zm)
 
         def end(self):
-            self.f0.wait_recv()
-            self.f1.wait_recv()
+            for c in (self.m0, self.p1, self.f0, self.f1):
+                c.wait_recv()
 
     def p1(r, h):
         return p.at[r, pl.ds(R1 // 2 * h, R1 // 2)]
@@ -291,8 +307,9 @@
                   yb0, yb1, yc0, yc1, yp, ym)
     z_out = Spread(R1, Q2, 64)
 
-    first_part(2)
-    y_first.far()
+    for h in (0, 1):
+        late(R1 // 2 * h, R1 // 2, xa)
+        y_first.far_half(h)
     for r in (2, 1, 3, 0):
         second_part(r)
     z_first.far()
@@ -301,7 +318,7 @@
     first_part(3)
     y_first.near()
 
-    lt[EARLY:TOK, :] = l[0:704, EARLY:TOK].T
+    lt[...] = l[0:704, :].T
 
     def token_grads(rel):
         rows = jnp.concatenate([lt[slot(k, rel):slot(k, rel) + ROWS, :] for k in range(4)], axis=0)
@@ -323,38 +340,34 @@
     x_ring.far()
     x_ring.near()
     first_part(0)
-
-    h0, h1 = z_first.end()
-    zr[:, 0:64, :] = h0.astype(BF16)
-    zr[:, 64:128, :] = h1.astype(BF16)
+    drain(14)
+
+    zr[:, 0:64, :] = z_first.end(0)
+    zr[:, 64:128, :] = z_first.end(1)
     z_then.far()
     z_then.near()
-    h0, h1 = y_first.end()
-    yr[0:R1 // 2, :] = h0.astype(BF16)
-    yr[R1 // 2:R1, :] = h1.astype(BF16)
+    yr[0:R1 // 2, :] = y_first.end(0)
+    yr[R1 // 2:R1, :] = y_first.end(1)
     y_then.far()
     y_then.near()
+    drain(8)
     x_ring.middle()
     z_then.middle()
     y_then.middle()
-    h0, h1 = z_then.end()
-    out[z_out_rows(z, 0), :] = h0.astype(BF16)
-    out[z_out_rows(z, 1), :] = h1.astype(BF16)
-    z_out.start()
-    h0, h1 = y_then.end()
-    out[q1(0, 0), :] = h0.astype(BF16)
-    out[q1(0, 1), :] = h1.astype(BF16)
-    y_out.start()
-    h0, h1 = x_ring.end()
-    gi_ref[0:48, :] = h0.astype(BF16)
-    gi_ref[48:96, :] = h1.astype(BF16)
+    for h in (0, 1):
+        out[z_out_rows(z, h), :] = z_then.end(h)
+        z_out.start(h)
+    for h in (0, 1):
+        out[q1(0, h), :] = y_then.end(h)
+        y_out.start(h)
+    drain(8)
+    gi_ref[0:48, :] = x_ring.end(0)
+    gi_ref[48:96, :] = x_ring.end(1)
     z_out.middle()
     y_out.middle()
     z_out.end()
     y_out.end()
-    dw_ref[...] = out[0:3 * HID, :]
-    for c in started:
-        c.wait_send()
+    drain()
 
 
 def z_out_rows(z, h):
@@ -381,7 +394,7 @@
     grad_in, sums = pl.pallas_call(
         kernel,
         name="ffn_backward",
-        out_shape=(pltpu.VMEM((ROWS, WIDTH), BF16), pltpu.VMEM((3 * HID, SHARD), BF16)),
+        out_shape=(pltpu.VMEM((ROWS, WIDTH), BF16), pltpu.VMEM((RP, SHARD), BF16)),
         in_specs=[pl.BlockSpec(memory_space=pl.ANY)] * 5,
         out_specs=(vmem, vmem),
         scratch_shapes=[
@@ -391,9 +404,8 @@
             pltpu.VMEM((3 * HID, EARLY), F32),
             pltpu.VMEM((RP, TOK), BF16),
             pltpu.VMEM((TOK, 2 * HID), BF16),
-            pltpu.VMEM((4, RP, SHARD), F32),
+            pltpu.VMEM((R1, SHARD), F32),
             pltpu.VMEM((4, RP, SHARD), BF16),
-            pltpu.VMEM((RP, SHARD), BF16),
             pltpu.VMEM((384, WIDTH), BF16),
             pltpu.VMEM((384, WIDTH), BF16),
             pltpu.VMEM((384, WIDTH), F32),
@@ -417,8 +429,8 @@
             pltpu.VMEM((64, SHARD), BF16),
             pltpu.VMEM((64, SHARD), BF16),
             pltpu.SemaphoreType.DMA((5,)),
-            pltpu.SemaphoreType.DMA((80,)),
-            pltpu.SemaphoreType.DMA((80,)),
+            pltpu.SemaphoreType.DMA((96,)),
+            pltpu.SemaphoreType.DMA((96,)),
         ],
         compiler_params=pltpu.CompilerParams(collective_id=0, has_side_effects=True),
     )(tokens_in, out_grad, gate_weight.T, up_weight.T, down_weight)

time: 56.1 us -> 55 us (0.980)
  Pallas kernels: 55.3 us -> 54.1 us
    pallas_call x1, Pallas kernels: 54.2 us -> 53 us  [body(): pl.pallas_call(kernel, name='ffn_backward', out_shape=(pltpu.VMEM((ROWS,...]
where the time goes in v3:
time: 55 us; the launch traced here: 54.8 us
  Pallas kernels  54.1 us (98%)
  between operations  0.64 us (1%)
    pallas_call x1, Pallas kernels, body(): pl.pallas_call(kernel, name='ffn_backward', out_shape=(pltpu.VMEM((ROWS,...  53 us

profile of v3, /device:TPU:0, one launch (start us, length us, event | category | flops | bytes accessed | tf_op | source)
XLA Modules:
  0.0 54.8 jit_solution(3756919132643048312)
XLA Ops:
  0.6 53.0 %ffn_backward.1 = (bf16[96,1024]{1,0:T(8,128)(2,1)S(1)}, bf16[1088,256]{1,0:T(8,128)(2,1)S(1)}) custom-call(bf16[96,1024]{1,0:T(8,128)(2,1)} %x_hbm.1, bf16[96,1024]{1,0:T(8,128)(2,1)} %o_hbm.1, bf16[352,256]{1,0:T(8,128)(2,1)} %bitcast.4, bf16[352,256]{1,0:T(8,128)(2,1)} %bitcast.5, bf16[352,256]{1,0:T(8,128)(2,1)} %d_hbm.1), custom_call_target="tpu_custom_call" | custom-call | tf_op jit(solution)/shard_map/ffn_backward/pallas_call | solution.py:394
  53.7 1.1 %finish.1 = (bf16[96,1024]{1,0:T(8,128)(2,1)}, f32[352,256]{1,0:T(8,128)}, f32[352,256]{1,0:T(8,128)}, f32[352,256]{1,0:T(8,128)}) custom-call(bf16[96,1024]{1,0:T(8,128)(2,1)S(1)} %get-tuple-element.10.gi_ref, bf16[1088,256]{1,0:T(8,128)(2,1)S(1)} %get-tuple-element.11.dw_ref), custom_call_target="tpu_custom_call" | custom-call | tf_op jit(solution)/shard_map/finish/pallas_call | solution.py:437

commit v4 on v3

--- a/solution.py
+++ b/solution.py
@@ -17,10 +17,10 @@
 SHARD = 256
 TOK = 768
 EARLY = 512
-R1 = 576
-R2 = 512
+R1 = 640
+R2 = 448
 RP = R1 + R2
-Q1, Q2 = R1 // 4, R2 // 4
+PIECE, Q2 = R1 // 4, R2 // 4
 
 
 def nt(a, b):
@@ -37,7 +37,7 @@
 
 def kernel(x_hbm, o_hbm, g_hbm, u_hbm, d_hbm, gi_ref, out,
            xa, oa, w, fwd, l, lt, pa, p, pb, rb, s0, sb, xr, xs,
-           ya, ys, yr, za0, za1, zs0, zs1, zb0, zb1, zc0, zc1, zr, yb0, yb1, yc0, yc1,
+           ya, ys, yr, got, half_sum, zb0, zb1, zc0, zc1, zr, yb0, yb1, yc0, yc1,
            ls, ss, rs):
     z = lax.axis_index("rep")
     y = lax.axis_index("fs")
@@ -170,15 +170,20 @@
     for c in (x_t, o_t, xt1, xt2, ot1, ot2):
         c.wait_recv()
 
-    def forward(c0, n):
+    def project(c0, n, parts=(0, 1, 2)):
         cols = pl.ds(c0, n)
-        for part, source in ((0, xa), (HID, xa), (2 * HID, oa)):
-            fwd[part:part + HID, 0:n] = nt(w[part:part + HID, :], source[cols, :])
+        for part in parts:
+            source = oa if part == 2 else xa
+            rows = pl.ds(HID * part, HID)
+            fwd[rows, cols] = nt(w[rows, :], source[cols, :])
+
+    def elementwise(c0, n):
+        cols = pl.ds(c0, n)
         for m in range(11):
             a = 32 * m
-            g = fwd[a:a + 32, 0:n].astype(BF16).astype(F32)
-            u = fwd[HID + a:HID + a + 32, 0:n].astype(BF16).astype(F32)
-            gh = fwd[2 * HID + a:2 * HID + a + 32, 0:n].astype(BF16).astype(F32)
+            g = fwd[a:a + 32, cols].astype(BF16).astype(F32)
+            u = fwd[HID + a:HID + a + 32, cols].astype(BF16).astype(F32)
+            gh = fwd[2 * HID + a:2 * HID + a + 32, cols].astype(BF16).astype(F32)
             sig = 1.0 / (1.0 + jnp.exp(-g))
             act = g * sig
             l[a:a + 32, cols] = (gh * u * sig * (1.0 + g * (1.0 - sig))).astype(BF16)
@@ -206,17 +211,23 @@
         whole(r, R1, 704 - R1, xa)
         whole(r, 704, RP - 704, oa)
 
-    forward(0, 256)
+    project(0, 256)
+    elementwise(0, 256)
     of_p.wait_recv()
     ot3 = send(tok(oa, slot(3, 0), 48), tok(oa, slot(3, 1), 48), twin)
     of_m.wait_recv()
     ot4 = send(tok(oa, slot(3, 0) + 48, 48), tok(oa, slot(3, 1) + 48, 48), twin)
-    forward(256, EARLY - 256)
+    project(256, EARLY - 256)
+    elementwise(256, EARLY - 256)
+    xt3.wait_recv()
+    xt4.wait_recv()
+    project(EARLY, TOK - EARLY, (0, 1))
     early(0, R1 // 2, xa)
     early(R1 // 2, R1 // 2, xa)
-    for c in (xt3, xt4, ot3, ot4):
-        c.wait_recv()
-    forward(EARLY, TOK - EARLY)
+    ot3.wait_recv()
+    ot4.wait_recv()
+    project(EARLY, TOK - EARLY, (2,))
+    elementwise(EARLY, TOK - EARLY)
 
     class Ring:
         def __init__(self, block, load, b0, b1, c0, c1, plus, minus):
@@ -289,20 +300,35 @@
     y_first = Ring(p1, lambda r, h: p[r, R1 // 2 * h:R1 // 2 * (h + 1), :],
                    ya.at[0], ya.at[1], ys.at[0], ys.at[1], yp, ym)
 
-    def q1(r, h):
-        return pl.ds(aligned(Q1 * lax.rem(z + r, 4) + 80 * h, 16), 64 if h else 80)
-
-    y_then = Ring(lambda r, h: yr.at[q1(r, h)], lambda r, h: yr[q1(r, h), :],
-                  za0, za1, zs0, zs1, zp, zm)
-    y_out = Spread(0, Q1, 80)
+    pair_a = (z + 1 - 2 * half, y, t)
+    pair_b = (lax.rem(z + 3 + 2 * half, 4), y, t)
+
+    class Exchange:
+        def __init__(self, i):
+            self.i, self.rows = i, pl.ds(PIECE * i, PIECE)
+            self.first, self.second = (pair_a, pair_b) if i < 2 else (pair_b, pair_a)
+
+        def start(self):
+            self.c0 = send(yr.at[self.rows], got.at[0, self.rows], self.first)
+
+        def middle(self):
+            self.c0.wait_recv()
+            half_sum[self.rows, :] = (yr[self.rows, :].astype(F32) + got[0, self.rows, :].astype(F32)).astype(BF16)
+            self.c1 = send(half_sum.at[self.rows], got.at[1, self.rows], self.second)
+
+        def end(self):
+            self.c1.wait_recv()
+            out[self.rows, :] = (half_sum[self.rows, :].astype(F32) + got[1, self.rows, :].astype(F32)).astype(BF16)
+
+    swaps = [Exchange(i) for i in range(4)]
 
     def q2(r, h):
-        return pl.ds(aligned(R1 + Q2 * lax.rem(z + r, 4) + 64 * h, 16), 64)
+        return pl.ds(aligned(R1 + Q2 * lax.rem(z + r, 4) + 64 * h, 16), 48 if h else 64)
 
     z_first = Ring(lambda r, h: p.at[:, q2(r, h)], lambda r, h: p[:, q2(r, h), :],
                    zb0, zb1, zc0, zc1, zp, zm)
     def zh(h):
-        return pl.ds(64 * h, 64)
+        return pl.ds(64 * h, 48 if h else 64)
     z_then = Ring(lambda r, h: zr.at[r, zh(h)], lambda r, h: zr[r, zh(h), :],
                   yb0, yb1, yc0, yc1, yp, ym)
     z_out = Spread(R1, Q2, 64)
@@ -343,35 +369,37 @@
     drain(14)
 
     zr[:, 0:64, :] = z_first.end(0)
-    zr[:, 64:128, :] = z_first.end(1)
+    zr[:, 64:112, :] = z_first.end(1)
     z_then.far()
     z_then.near()
     yr[0:R1 // 2, :] = y_first.end(0)
+    swaps[0].start()
+    swaps[1].start()
     yr[R1 // 2:R1, :] = y_first.end(1)
-    y_then.far()
-    y_then.near()
+    swaps[2].start()
+    swaps[3].start()
     drain(8)
     x_ring.middle()
     z_then.middle()
-    y_then.middle()
+    for i in (0, 2):
+        swaps[i].middle()
     for h in (0, 1):
         out[z_out_rows(z, h), :] = z_then.end(h)
         z_out.start(h)
-    for h in (0, 1):
-        out[q1(0, h), :] = y_then.end(h)
-        y_out.start(h)
+    for i in (1, 3):
+        swaps[i].middle()
     drain(8)
     gi_ref[0:48, :] = x_ring.end(0)
     gi_ref[48:96, :] = x_ring.end(1)
     z_out.middle()
-    y_out.middle()
+    for i in (0, 2, 1, 3):
+        swaps[i].end()
     z_out.end()
-    y_out.end()
     drain()
 
 
 def z_out_rows(z, h):
-    return pl.ds(pl.multiple_of(R1 + Q2 * z + 64 * h, 16), 64)
+    return pl.ds(pl.multiple_of(R1 + Q2 * z + 64 * h, 16), 48 if h else 64)
 
 
 def finish(factor, gi_ref, dw_ref, gi_hbm, og_hbm, ou_hbm, od_hbm, gi, og, ou, od, sems):
@@ -401,7 +429,7 @@
             pltpu.VMEM((TOK, WIDTH), BF16),
             pltpu.VMEM((TOK, WIDTH), BF16),
             pltpu.VMEM((3 * HID, WIDTH), BF16),
-            pltpu.VMEM((3 * HID, EARLY), F32),
+            pltpu.VMEM((3 * HID, TOK), F32),
             pltpu.VMEM((RP, TOK), BF16),
             pltpu.VMEM((TOK, 2 * HID), BF16),
             pltpu.VMEM((R1, SHARD), F32),
@@ -415,19 +443,17 @@
             pltpu.VMEM((2, 3, R1 // 2, SHARD), BF16),
             pltpu.VMEM((2, R1 // 2, SHARD), BF16),
             pltpu.VMEM((R1, SHARD), BF16),
-            pltpu.VMEM((3, 80, SHARD), BF16),
-            pltpu.VMEM((3, 64, SHARD), BF16),
-            pltpu.VMEM((80, SHARD), BF16),
-            pltpu.VMEM((64, SHARD), BF16),
+            pltpu.VMEM((2, R1, SHARD), BF16),
+            pltpu.VMEM((R1, SHARD), BF16),
             pltpu.VMEM((3, 4, 64, SHARD), BF16),
-            pltpu.VMEM((3, 4, 64, SHARD), BF16),
+            pltpu.VMEM((3, 4, 48, SHARD), BF16),
             pltpu.VMEM((4, 64, SHARD), BF16),
-            pltpu.VMEM((4, 64, SHARD), BF16),
+            pltpu.VMEM((4, 48, SHARD), BF16),
             pltpu.VMEM((4, Q2, SHARD), BF16),
             pltpu.VMEM((3, 64, SHARD), BF16),
-            pltpu.VMEM((3, 64, SHARD), BF16),
+            pltpu.VMEM((3, 48, SHARD), BF16),
             pltpu.VMEM((64, SHARD), BF16),
-            pltpu.VMEM((64, SHARD), BF16),
+            pltpu.VMEM((48, SHARD), BF16),
             pltpu.SemaphoreType.DMA((5,)),
             pltpu.SemaphoreType.DMA((96,)),
             pltpu.SemaphoreType.DMA((96,)),

time: 55 us -> 54.2 us (0.985)
  Pallas kernels: 54.1 us -> 53.4 us
    pallas_call x1, Pallas kernels: 53 us -> 52.4 us  [body(): pl.pallas_call(kernel, name='ffn_backward', out_shape=(pltpu.VMEM((ROWS,...]
where the time goes in v4:
time: 54.2 us; the launch traced here: 54.1 us
  Pallas kernels  53.4 us (99%)
  between operations  0.64 us (1%)
    pallas_call x1, Pallas kernels, body(): pl.pallas_call(kernel, name='ffn_backward', out_shape=(pltpu.VMEM((ROWS,...  52.4 us
    pallas_call x1, Pallas kernels, body(): pl.pallas_call(functools.partial(finish, factor), name='finish', out_shap...  1.09 us

profile of v4, /device:TPU:0, one launch (start us, length us, event | category | flops | bytes accessed | tf_op | source)
XLA Modules:
  0.0 54.1 jit_solution(10450443675408513910)
XLA Ops:
  0.6 52.4 %ffn_backward.1 = (bf16[96,1024]{1,0:T(8,128)(2,1)S(1)}, bf16[1088,256]{1,0:T(8,128)(2,1)S(1)}) custom-call(bf16[96,1024]{1,0:T(8,128)(2,1)} %x_hbm.1, bf16[96,1024]{1,0:T(8,128)(2,1)} %o_hbm.1, bf16[352,256]{1,0:T(8,128)(2,1)} %bitcast.4, bf16[352,256]{1,0:T(8,128)(2,1)} %bitcast.5, bf16[352,256]{1,0:T(8,128)(2,1)} %d_hbm.1), custom_call_target="tpu_custom_call" | custom-call | tf_op jit(solution)/shard_map/ffn_backward/pallas_call | solution.py:422
  53.0 1.1 %finish.1 = (bf16[96,1024]{1,0:T(8,128)(2,1)}, f32[352,256]{1,0:T(8,128)}, f32[352,256]{1,0:T(8,128)}, f32[352,256]{1,0:T(8,128)}) custom-call(bf16[96,1024]{1,0:T(8,128)(2,1)S(1)} %get-tuple-element.10.gi_ref, bf16[1088,256]{1,0:T(8,128)(2,1)S(1)} %get-tuple-element.11.dw_ref), custom_call_target="tpu_custom_call" | custom-call | tf_op jit(solution)/shard_map/finish/pallas_call | solution.py:463

commit v5 on v4

--- a/solution.py
+++ b/solution.py
@@ -17,10 +17,11 @@
 SHARD = 256
 TOK = 768
 EARLY = 512
-R1 = 640
-R2 = 448
+R1 = 576
+R2 = 512
 RP = R1 + R2
 PIECE, Q2 = R1 // 4, R2 // 4
+H0, H1 = 64, 64
 
 
 def nt(a, b):
@@ -36,7 +37,7 @@
 
 
 def kernel(x_hbm, o_hbm, g_hbm, u_hbm, d_hbm, gi_ref, out,
-           xa, oa, w, fwd, l, lt, pa, p, pb, rb, s0, sb, xr, xs,
+           xa, oa, w, fwd, l, lt, pa, pz, p, pb, rb, s0, sb, xr, xs,
            ya, ys, yr, got, half_sum, zb0, zb1, zc0, zc1, zr, yb0, yb1, yc0, yc1,
            ls, ss, rs):
     z = lax.axis_index("rep")
@@ -203,13 +204,19 @@
     def whole(r, row, n, source):
         p[r, row:row + n, :] = nn(l[row:row + n, :], source[:, shard_cols(r)]).astype(BF16)
 
+    def early_second(r):
+        pz[r, 0:704 - R1, :] = nn(l[R1:704, 0:EARLY], xa[0:EARLY, shard_cols(r)])
+        pz[r, 704 - R1:R2, :] = nn(l[704:RP, 0:EARLY], oa[0:EARLY, shard_cols(r)])
+
     def first_part(r):
         whole(r, 0, R1 // 2, xa)
         whole(r, R1 // 2, R1 // 2, xa)
 
     def second_part(r):
-        whole(r, R1, 704 - R1, xa)
-        whole(r, 704, RP - 704, oa)
+        more = nn(l[R1:704, EARLY:TOK], xa[EARLY:TOK, shard_cols(r)])
+        p[r, R1:704, :] = (pz[r, 0:704 - R1, :] + more).astype(BF16)
+        more = nn(l[704:RP, EARLY:TOK], oa[EARLY:TOK, shard_cols(r)])
+        p[r, 704:RP, :] = (pz[r, 704 - R1:R2, :] + more).astype(BF16)
 
     project(0, 256)
     elementwise(0, 256)
@@ -224,6 +231,8 @@
     project(EARLY, TOK - EARLY, (0, 1))
     early(0, R1 // 2, xa)
     early(R1 // 2, R1 // 2, xa)
+    for r in (2, 1, 3, 0):
+        early_second(r)
     ot3.wait_recv()
     ot4.wait_recv()
     project(EARLY, TOK - EARLY, (2,))
@@ -323,15 +332,15 @@
     swaps = [Exchange(i) for i in range(4)]
 
     def q2(r, h):
-        return pl.ds(aligned(R1 + Q2 * lax.rem(z + r, 4) + 64 * h, 16), 48 if h else 64)
+        return pl.ds(aligned(R1 + Q2 * lax.rem(z + r, 4) + H0 * h, 16), H1 if h else H0)
 
     z_first = Ring(lambda r, h: p.at[:, q2(r, h)], lambda r, h: p[:, q2(r, h), :],
                    zb0, zb1, zc0, zc1, zp, zm)
     def zh(h):
-        return pl.ds(64 * h, 48 if h else 64)
+        return pl.ds(H0 * h, H1 if h else H0)
     z_then = Ring(lambda r, h: zr.at[r, zh(h)], lambda r, h: zr[r, zh(h), :],
                   yb0, yb1, yc0, yc1, yp, ym)
-    z_out = Spread(R1, Q2, 64)
+    z_out = Spread(R1, Q2, H0)
 
     for h in (0, 1):
         late(R1 // 2 * h, R1 // 2, xa)
@@ -368,8 +377,8 @@
     first_part(0)
     drain(14)
 
-    zr[:, 0:64, :] = z_first.end(0)
-    zr[:, 64:112, :] = z_first.end(1)
+    zr[:, 0:H0, :] = z_first.end(0)
+    zr[:, H0:Q2, :] = z_first.end(1)
     z_then.far()
     z_then.near()
     yr[0:R1 // 2, :] = y_first.end(0)
@@ -381,12 +390,10 @@
     drain(8)
     x_ring.middle()
     z_then.middle()
-    for i in (0, 2):
-        swaps[i].middle()
     for h in (0, 1):
         out[z_out_rows(z, h), :] = z_then.end(h)
         z_out.start(h)
-    for i in (1, 3):
+    for i in (0, 2, 1, 3):
         swaps[i].middle()
     drain(8)
     gi_ref[0:48, :] = x_ring.end(0)
@@ -399,7 +406,7 @@
 
 
 def z_out_rows(z, h):
-    return pl.ds(pl.multiple_of(R1 + Q2 * z + 64 * h, 16), 48 if h else 64)
+    return pl.ds(pl.multiple_of(R1 + Q2 * z + H0 * h, 16), H1 if h else H0)
 
 
 def finish(factor, gi_ref, dw_ref, gi_hbm, og_hbm, ou_hbm, od_hbm, gi, og, ou, od, sems):
@@ -433,6 +440,7 @@
             pltpu.VMEM((RP, TOK), BF16),
             pltpu.VMEM((TOK, 2 * HID), BF16),
             pltpu.VMEM((R1, SHARD), F32),
+            pltpu.VMEM((4, R2, SHARD), F32),
             pltpu.VMEM((4, RP, SHARD), BF16),
             pltpu.VMEM((384, WIDTH), BF16),
             pltpu.VMEM((384, WIDTH), BF16),
@@ -445,15 +453,15 @@
             pltpu.VMEM((R1, SHARD), BF16),
             pltpu.VMEM((2, R1, SHARD), BF16),
             pltpu.VMEM((R1, SHARD), BF16),
-            pltpu.VMEM((3, 4, 64, SHARD), BF16),
-            pltpu.VMEM((3, 4, 48, SHARD), BF16),
-            pltpu.VMEM((4, 64, SHARD), BF16),
-            pltpu.VMEM((4, 48, SHARD), BF16),
+            pltpu.VMEM((3, 4, H0, SHARD), BF16),
+            pltpu.VMEM((3, 4, H1, SHARD), BF16),
+            pltpu.VMEM((4, H0, SHARD), BF16),
+            pltpu.VMEM((4, H1, SHARD), BF16),
             pltpu.VMEM((4, Q2, SHARD), BF16),
-            pltpu.VMEM((3, 64, SHARD), BF16),
-            pltpu.VMEM((3, 48, SHARD), BF16),
-            pltpu.VMEM((64, SHARD), BF16),
-            pltpu.VMEM((48, SHARD), BF16),
+            pltpu.VMEM((3, H0, SHARD), BF16),
+            pltpu.VMEM((3, H1, SHARD), BF16),
+            pltpu.VMEM((H0, SHARD), BF16),
+            pltpu.VMEM((H1, SHARD), BF16),
             pltpu.SemaphoreType.DMA((5,)),
             pltpu.SemaphoreType.DMA((96,)),
             pltpu.SemaphoreType.DMA((96,)),

time: 54.2 us -> 52.7 us (0.972)
  Pallas kernels: 53.4 us -> 51.9 us
    pallas_call x1, Pallas kernels: 52.4 us -> 50.8 us  [body(): pl.pallas_call(kernel, name='ffn_backward', out_shape=(pltpu.VMEM((ROWS,...]
where the time goes in v5:
time: 52.7 us; the launch traced here: 52.6 us
  Pallas kernels  51.9 us (98%)
  between operations  0.64 us (1%)
    pallas_call x1, Pallas kernels, body(): pl.pallas_call(kernel, name='ffn_backward', out_shape=(pltpu.VMEM((ROWS,...  50.8 us
    pallas_call x1, Pallas kernels, body(): pl.pallas_call(functools.partial(finish, factor), name='finish', out_shap...  1.09 us

profile of v5, /device:TPU:0, one launch (start us, length us, event | category | flops | bytes accessed | tf_op | source)
XLA Modules:
  0.0 52.6 jit_solution(7058780169882446421)
XLA Ops:
  0.6 50.8 %ffn_backward.1 = (bf16[96,1024]{1,0:T(8,128)(2,1)S(1)}, bf16[1088,256]{1,0:T(8,128)(2,1)S(1)}) custom-call(bf16[96,1024]{1,0:T(8,128)(2,1)} %x_hbm.1, bf16[96,1024]{1,0:T(8,128)(2,1)} %o_hbm.1, bf16[352,256]{1,0:T(8,128)(2,1)} %bitcast.4, bf16[352,256]{1,0:T(8,128)(2,1)} %bitcast.5, bf16[352,256]{1,0:T(8,128)(2,1)} %d_hbm.1), custom_call_target="tpu_custom_call" | custom-call | tf_op jit(solution)/shard_map/ffn_backward/pallas_call | solution.py:429
  51.5 1.1 %finish.1 = (bf16[96,1024]{1,0:T(8,128)(2,1)}, f32[352,256]{1,0:T(8,128)}, f32[352,256]{1,0:T(8,128)}, f32[352,256]{1,0:T(8,128)}) custom-call(bf16[96,1024]{1,0:T(8,128)(2,1)S(1)} %get-tuple-element.10.gi_ref, bf16[1088,256]{1,0:T(8,128)(2,1)S(1)} %get-tuple-element.11.dw_ref), custom_call_target="tpu_custom_call" | custom-call | tf_op jit(solution)/shard_map/finish/pallas_call | solution.py:471

commit v6 on v5

--- a/solution.py
+++ b/solution.py
@@ -22,6 +22,9 @@
 RP = R1 + R2
 PIECE, Q2 = R1 // 4, R2 // 4
 H0, H1 = 64, 64
+
+
+AT = (3, 0, 1, 2)
 
 
 def nt(a, b):
@@ -199,10 +202,10 @@
 
     def late(row, n, source):
         more = nn(l[row:row + n, EARLY:TOK], source[EARLY:TOK, shard_cols(2)])
-        p[2, row:row + n, :] = (pa[row:row + n, :] + more).astype(BF16)
+        p[AT[2], row:row + n, :] = (pa[row:row + n, :] + more).astype(BF16)
 
     def whole(r, row, n, source):
-        p[r, row:row + n, :] = nn(l[row:row + n, :], source[:, shard_cols(r)]).astype(BF16)
+        p[AT[r], row:row + n, :] = nn(l[row:row + n, :], source[:, shard_cols(r)]).astype(BF16)
 
     def early_second(r):
         pz[r, 0:704 - R1, :] = nn(l[R1:704, 0:EARLY], xa[0:EARLY, shard_cols(r)])
@@ -214,9 +217,9 @@
 
     def second_part(r):
         more = nn(l[R1:704, EARLY:TOK], xa[EARLY:TOK, shard_cols(r)])
-        p[r, R1:704, :] = (pz[r, 0:704 - R1, :] + more).astype(BF16)
+        p[AT[r], R1:704, :] = (pz[r, 0:704 - R1, :] + more).astype(BF16)
         more = nn(l[704:RP, EARLY:TOK], oa[EARLY:TOK, shard_cols(r)])
-        p[r, 704:RP, :] = (pz[r, 704 - R1:R2, :] + more).astype(BF16)
+        p[AT[r], 704:RP, :] = (pz[r, 704 - R1:R2, :] + more).astype(BF16)
 
     project(0, 256)
     elementwise(0, 256)
@@ -255,8 +258,14 @@
                 self.a0 = send(self.block(2, 0), self.b0.at[0], self.plus)
 
         def near(self):
-            self.n1 = send(self.block(1, 1), self.b1.at[1], self.plus)
-            self.n0 = send(self.block(3, 0), self.b0.at[1], self.minus)
+            self.near_half(1)
+            self.near_half(0)
+
+        def near_half(self, h):
+            if h:
+                self.n1 = send(self.block(1, 1), self.b1.at[1], self.plus)
+            else:
+                self.n0 = send(self.block(3, 0), self.b0.at[1], self.minus)
 
         def middle(self):
             self.a0.wait_recv()
@@ -303,11 +312,13 @@
             for c in (self.m0, self.p1, self.f0, self.f1):
                 c.wait_recv()
 
-    def p1(r, h):
-        return p.at[r, pl.ds(R1 // 2 * h, R1 // 2)]
-
-    y_first = Ring(p1, lambda r, h: p[r, R1 // 2 * h:R1 // 2 * (h + 1), :],
-                   ya.at[0], ya.at[1], ys.at[0], ys.at[1], yp, ym)
+    def y_ring(k):
+        def rows(h):
+            return pl.ds(R1 // 2 * h + PIECE * k, PIECE)
+        return Ring(lambda r, h: p.at[AT[r], rows(h)], lambda r, h: p[AT[r], rows(h), :],
+                    ya.at[k, 0], ya.at[k, 1], ys.at[k, 0], ys.at[k, 1], yp, ym)
+
+    y_first = [y_ring(0), y_ring(1)]
 
     pair_a = (z + 1 - 2 * half, y, t)
     pair_b = (lax.rem(z + 3 + 2 * half, 4), y, t)
@@ -334,24 +345,33 @@
     def q2(r, h):
         return pl.ds(aligned(R1 + Q2 * lax.rem(z + r, 4) + H0 * h, 16), H1 if h else H0)
 
-    z_first = Ring(lambda r, h: p.at[:, q2(r, h)], lambda r, h: p[:, q2(r, h), :],
-                   zb0, zb1, zc0, zc1, zp, zm)
+    def z_ring(k):
+        two = pl.ds(2 * k, 2)
+        return Ring(lambda r, h: p.at[two, q2(r, h)], lambda r, h: p[two, q2(r, h), :],
+                    zb0.at[k], zb1.at[k], zc0.at[k], zc1.at[k], zp, zm)
+
+    z_first = [z_ring(0), z_ring(1)]
+
     def zh(h):
         return pl.ds(H0 * h, H1 if h else H0)
-    z_then = Ring(lambda r, h: zr.at[r, zh(h)], lambda r, h: zr[r, zh(h), :],
+    z_then = Ring(lambda r, h: zr.at[AT[r], zh(h)], lambda r, h: zr[AT[r], zh(h), :],
                   yb0, yb1, yc0, yc1, yp, ym)
     z_out = Spread(R1, Q2, H0)
 
     for h in (0, 1):
         late(R1 // 2 * h, R1 // 2, xa)
-        y_first.far_half(h)
+        y_first[0].far_half(h)
+        y_first[1].far_half(h)
     for r in (2, 1, 3, 0):
         second_part(r)
-    z_first.far()
-    z_first.near()
+    z_first[0].far()
+    z_first[1].far()
+    z_first[0].near()
+    z_first[1].near()
     first_part(1)
     first_part(3)
-    y_first.near()
+    y_first[0].near()
+    y_first[1].near()
 
     lt[...] = l[0:704, :].T
 
@@ -363,8 +383,10 @@
     pair = send(pb, rb, twin)
     s0[...] = token_grads(0)
 
-    y_first.middle()
-    z_first.middle()
+    y_first[0].middle()
+    z_first[0].middle()
+    y_first[1].middle()
+    z_first[1].middle()
     pair.wait_recv()
     sb[...] = (s0[...] + rb[...].astype(F32)).astype(BF16)
     chip = {0: 0, 3: 1, 1: 2, 2: 3}
@@ -375,18 +397,20 @@
     x_ring.far()
     x_ring.near()
     first_part(0)
-    drain(14)
-
-    zr[:, 0:H0, :] = z_first.end(0)
-    zr[:, H0:Q2, :] = z_first.end(1)
+    drain(16)
+
+    for h in (0, 1):
+        zr[0:2, zh(h), :] = z_first[0].end(h)
     z_then.far()
-    z_then.near()
-    yr[0:R1 // 2, :] = y_first.end(0)
-    swaps[0].start()
-    swaps[1].start()
-    yr[R1 // 2:R1, :] = y_first.end(1)
-    swaps[2].start()
-    swaps[3].start()
+    z_then.near_half(1)
+    for k in (0, 1):
+        for h in (0, 1):
+            yr[pl.ds(R1 // 2 * h + PIECE * k, PIECE), :] = y_first[k].end(h)
+            swaps[2 * h + k].start()
+        if k == 0:
+            for h in (0, 1):
+                zr[2:4, zh(h), :] = z_first[1].end(h)
+            z_then.near_half(0)
     drain(8)
     x_ring.middle()
     z_then.middle()
@@ -448,23 +472,23 @@
             pltpu.VMEM((384, WIDTH), BF16),
             pltpu.VMEM((2, 3, 48, WIDTH), BF16),
             pltpu.VMEM((2, 48, WIDTH), BF16),
-            pltpu.VMEM((2, 3, R1 // 2, SHARD), BF16),
-            pltpu.VMEM((2, R1 // 2, SHARD), BF16),
+            pltpu.VMEM((2, 2, 3, PIECE, SHARD), BF16),
+            pltpu.VMEM((2, 2, PIECE, SHARD), BF16),
             pltpu.VMEM((R1, SHARD), BF16),
             pltpu.VMEM((2, R1, SHARD), BF16),
             pltpu.VMEM((R1, SHARD), BF16),
-            pltpu.VMEM((3, 4, H0, SHARD), BF16),
-            pltpu.VMEM((3, 4, H1, SHARD), BF16),
-            pltpu.VMEM((4, H0, SHARD), BF16),
-            pltpu.VMEM((4, H1, SHARD), BF16),
+            pltpu.VMEM((2, 3, 2, H0, SHARD), BF16),
+            pltpu.VMEM((2, 3, 2, H1, SHARD), BF16),
+            pltpu.VMEM((2, 2, H0, SHARD), BF16),
+            pltpu.VMEM((2, 2, H1, SHARD), BF16),
             pltpu.VMEM((4, Q2, SHARD), BF16),
             pltpu.VMEM((3, H0, SHARD), BF16),
             pltpu.VMEM((3, H1, SHARD), BF16),
             pltpu.VMEM((H0, SHARD), BF16),
             pltpu.VMEM((H1, SHARD), BF16),
             pltpu.SemaphoreType.DMA((5,)),
-            pltpu.SemaphoreType.DMA((96,)),
-            pltpu.SemaphoreType.DMA((96,)),
+            pltpu.SemaphoreType.DMA((112,)),
+            pltpu.SemaphoreType.DMA((112,)),
         ],
         compiler_params=pltpu.CompilerParams(collective_id=0, has_side_effects=True),
     )(tokens_in, out_grad, gate_weight.T, up_weight.T, down_weight)

time: 52.7 us -> 51.9 us (0.985)
  Pallas kernels: 51.9 us -> 50.8 us
    pallas_call x1, Pallas kernels: 50.8 us -> 49.7 us  [body(): pl.pallas_call(kernel, name='ffn_backward', out_shape=(pltpu.VMEM((ROWS,...]
where the time goes in v6:
time: 51.9 us; the launch traced here: 51.4 us
  Pallas kernels  50.8 us (98%)
  between operations  0.64 us (1%)
    pallas_call x1, Pallas kernels, body(): pl.pallas_call(kernel, name='ffn_backward', out_shape=(pltpu.VMEM((ROWS,...  49.7 us
    pallas_call x1, Pallas kernels, body(): pl.pallas_call(functools.partial(finish, factor), name='finish', out_shap...  1.09 us

profile of v6, /device:TPU:0, one launch (start us, length us, event | category | flops | bytes accessed | tf_op | source)
XLA Modules:
  0.0 51.4 jit_solution(10516578100638806981)
XLA Ops:
  0.6 49.7 %ffn_backward.1 = (bf16[96,1024]{1,0:T(8,128)(2,1)S(1)}, bf16[1088,256]{1,0:T(8,128)(2,1)S(1)}) custom-call(bf16[96,1024]{1,0:T(8,128)(2,1)} %x_hbm.1, bf16[96,1024]{1,0:T(8,128)(2,1)} %o_hbm.1, bf16[352,256]{1,0:T(8,128)(2,1)} %bitcast.4, bf16[352,256]{1,0:T(8,128)(2,1)} %bitcast.5, bf16[352,256]{1,0:T(8,128)(2,1)} %d_hbm.1), custom_call_target="tpu_custom_call" | custom-call | tf_op jit(solution)/shard_map/ffn_backward/pallas_call | solution.py:453
  50.3 1.1 %finish.1 = (bf16[96,1024]{1,0:T(8,128)(2,1)}, f32[352,256]{1,0:T(8,128)}, f32[352,256]{1,0:T(8,128)}, f32[352,256]{1,0:T(8,128)}) custom-call(bf16[96,1024]{1,0:T(8,128)(2,1)S(1)} %get-tuple-element.10.gi_ref, bf16[1088,256]{1,0:T(8,128)(2,1)S(1)} %get-tuple-element.11.dw_ref), custom_call_target="tpu_custom_call" | custom-call | tf_op jit(solution)/shard_map/finish/pallas_call | solution.py:495

commit v7 on v6

--- a/solution.py
+++ b/solution.py
@@ -178,8 +178,9 @@
         cols = pl.ds(c0, n)
         for part in parts:
             source = oa if part == 2 else xa
-            rows = pl.ds(HID * part, HID)
-            fwd[rows, cols] = nt(w[rows, :], source[cols, :])
+            for m in (0, 1):
+                rows = pl.ds(HID * part + HID // 2 * m, HID // 2)
+                fwd[rows, cols] = nt(w[rows, :], source[cols, :])
 
     def elementwise(c0, n):
         cols = pl.ds(c0, n)

time: 51.9 us -> 51.7 us (level)
  no operation moved by 1% of the time
where the time goes in v7:
time: 51.7 us; the launch traced here: 51.5 us
  Pallas kernels  50.9 us (98%)
  between operations  0.64 us (1%)
    pallas_call x1, Pallas kernels, body(): pl.pallas_call(kernel, name='ffn_backward', out_shape=(pltpu.VMEM((ROWS,...  49.8 us
    pallas_call x1, Pallas kernels, body(): pl.pallas_call(functools.partial(finish, factor), name='finish', out_shap...  1.09 us

profile of v7, /device:TPU:0, one launch (start us, length us, event | category | flops | bytes accessed | tf_op | source)
XLA Modules:
  0.0 51.5 jit_solution(9453053108335632915)
XLA Ops:
  0.6 49.8 %ffn_backward.1 = (bf16[96,1024]{1,0:T(8,128)(2,1)S(1)}, bf16[1088,256]{1,0:T(8,128)(2,1)S(1)}) custom-call(bf16[96,1024]{1,0:T(8,128)(2,1)} %x_hbm.1, bf16[96,1024]{1,0:T(8,128)(2,1)} %o_hbm.1, bf16[352,256]{1,0:T(8,128)(2,1)} %bitcast.4, bf16[352,256]{1,0:T(8,128)(2,1)} %bitcast.5, bf16[352,256]{1,0:T(8,128)(2,1)} %d_hbm.1), custom_call_target="tpu_custom_call" | custom-call | tf_op jit(solution)/shard_map/ffn_backward/pallas_call | solution.py:454
  50.4 1.1 %finish.1 = (bf16[96,1024]{1,0:T(8,128)(2,1)}, f32[352,256]{1,0:T(8,128)}, f32[352,256]{1,0:T(8,128)}, f32[352,256]{1,0:T(8,128)}) custom-call(bf16[96,1024]{1,0:T(8,128)(2,1)S(1)} %get-tuple-element.10.gi_ref, bf16[1088,256]{1,0:T(8,128)(2,1)S(1)} %get-tuple-element.11.dw_ref), custom_call_target="tpu_custom_call" | custom-call | tf_op jit(solution)/shard_map/finish/pallas_call | solution.py:496

commit v8 on v7

--- a/solution.py
+++ b/solution.py
@@ -96,7 +96,7 @@
     def tok(ref, row, n):
         return ref.at[pl.ds(row, n)]
 
-    my_rows = [aligned(640 * half, 16), aligned(640 * half + 208, 16), 416]
+    my_rows = [aligned(608 * half, 16), aligned(608 * half + 224, 16), 448]
 
     def wblk(row, n, col):
         return w.at[pl.ds(row, n), pl.ds(aligned(lax.rem(col, 4) * SHARD, SHARD), SHARD)]
@@ -112,10 +112,10 @@
     x_t = send(tok(xa, 0, ROWS), tok(xa, slot(0, 1), ROWS), twin)
     for c in locals_[1:4]:
         c.wait()
-    wp_a = wsend(0, 0, 208, y, yp)
-    wm_b = wsend(1, 0, 208, y, ym)
-    wp_b = wsend(1, 0, 208, y, yp)
-    wm_a = wsend(0, 0, 208, y, ym)
+    wp_a = wsend(0, 0, 224, y, yp)
+    wm_b = wsend(1, 0, 224, y, ym)
+    wp_b = wsend(1, 0, 224, y, yp)
+    wm_a = wsend(0, 0, 224, y, ym)
     locals_[4].wait()
     o_p = send(tok(oa, 0, ROWS), tok(oa, slot(1, 0), ROWS), xp)
     o_m = send(tok(oa, 0, ROWS), tok(oa, slot(2, 0), ROWS), xm)
@@ -124,16 +124,16 @@
     z_in = []
 
     def zsend(i, col, dev):
-        z_in.append(wsend(i, 0, 208, col, dev))
+        z_in.append(wsend(i, 0, 224, col, dev))
 
     wp_a.wait_recv()
-    fp_a = wsend(0, 0, 208, y + 3, yp)
+    fp_a = wsend(0, 0, 224, y + 3, yp)
     zsend(0, y + 3, zp)
     wm_b.wait_recv()
-    fm_b = wsend(1, 0, 208, y + 1, ym)
+    fm_b = wsend(1, 0, 224, y + 1, ym)
     zsend(1, y + 1, zm)
-    wp_c = wsend(2, 0, 224, y, yp)
-    wm_c = wsend(2, 0, 224, y, ym)
+    wp_c = wsend(2, 0, 160, y, yp)
+    wm_c = wsend(2, 0, 160, y, ym)
 
     x_p.wait_recv()
     xf_p = send(tok(xa, slot(1, 0), 48), tok(xa, slot(3, 0), 48), xp)
@@ -152,9 +152,9 @@
     zsend(1, y + 2, zm)
 
     wp_c.wait_recv()
-    fp_c = wsend(2, 0, 112, y + 3, yp)
+    fp_c = wsend(2, 0, 80, y + 3, yp)
     wm_c.wait_recv()
-    fm_c = wsend(2, 112, 112, y + 1, ym)
+    fm_c = wsend(2, 80, 80, y + 1, ym)
 
     o_p.wait_recv()
     of_p = send(tok(oa, slot(1, 0), 48), tok(oa, slot(3, 0), 48), xp)
@@ -412,7 +412,7 @@
             for h in (0, 1):
                 zr[2:4, zh(h), :] = z_first[1].end(h)
             z_then.near_half(0)
-    drain(8)
+    drain(20)
     x_ring.middle()
     z_then.middle()
     for h in (0, 1):

time: 51.7 us -> 51.5 us (level)
  no operation moved by 1% of the time
where the time goes in v8:
time: 51.5 us; the launch traced here: 51.4 us
  Pallas kernels  50.8 us (99%)
  between operations  0.64 us (1%)
    pallas_call x1, Pallas kernels, body(): pl.pallas_call(kernel, name='ffn_backward', out_shape=(pltpu.VMEM((ROWS,...  49.7 us
    pallas_call x1, Pallas kernels, body(): pl.pallas_call(functools.partial(finish, factor), name='finish', out_shap...  1.09 us

profile of v8, /device:TPU:0, one launch (start us, length us, event | category | flops | bytes accessed | tf_op | source)
XLA Modules:
  0.0 51.4 jit_solution(2755469714653156539)
XLA Ops:
  0.6 49.7 %ffn_backward.1 = (bf16[96,1024]{1,0:T(8,128)(2,1)S(1)}, bf16[1088,256]{1,0:T(8,128)(2,1)S(1)}) custom-call(bf16[96,1024]{1,0:T(8,128)(2,1)} %x_hbm.1, bf16[96,1024]{1,0:T(8,128)(2,1)} %o_hbm.1, bf16[352,256]{1,0:T(8,128)(2,1)} %bitcast.4, bf16[352,256]{1,0:T(8,128)(2,1)} %bitcast.5, bf16[352,256]{1,0:T(8,128)(2,1)} %d_hbm.1), custom_call_target="tpu_custom_call" | custom-call | tf_op jit(solution)/shard_map/ffn_backward/pallas_call | solution.py:454
  50.3 1.1 %finish.1 = (bf16[96,1024]{1,0:T(8,128)(2,1)}, f32[352,256]{1,0:T(8,128)}, f32[352,256]{1,0:T(8,128)}, f32[352,256]{1,0:T(8,128)}) custom-call(bf16[96,1024]{1,0:T(8,128)(2,1)S(1)} %get-tuple-element.10.gi_ref, bf16[1088,256]{1,0:T(8,128)(2,1)S(1)} %get-tuple-element.11.dw_ref), custom_call_target="tpu_custom_call" | custom-call | tf_op jit(solution)/shard_map/finish/pallas_call | solution.py:496

commit v9 on v8

--- a/solution.py
+++ b/solution.py
@@ -189,7 +189,7 @@
             g = fwd[a:a + 32, cols].astype(BF16).astype(F32)
             u = fwd[HID + a:HID + a + 32, cols].astype(BF16).astype(F32)
             gh = fwd[2 * HID + a:2 * HID + a + 32, cols].astype(BF16).astype(F32)
-            sig = 1.0 / (1.0 + jnp.exp(-g))
+            sig = jax.nn.sigmoid(g)
             act = g * sig
             l[a:a + 32, cols] = (gh * u * sig * (1.0 + g * (1.0 - sig))).astype(BF16)
             l[HID + a:HID + a + 32, cols] = (gh * act).astype(BF16)
@@ -382,9 +382,9 @@
 
     pb[...] = token_grads(1).astype(BF16)
     pair = send(pb, rb, twin)
+    y_first[0].middle()
     s0[...] = token_grads(0)
 
-    y_first[0].middle()
     z_first[0].middle()
     y_first[1].middle()
     z_first[1].middle()

time: 51.5 us -> 51.5 us (level)
  no operation moved by 1% of the time
where the time goes in v9:
time: 51.5 us; the launch traced here: 51.4 us
  Pallas kernels  50.8 us (99%)
  between operations  0.64 us (1%)
    pallas_call x1, Pallas kernels, body(): pl.pallas_call(kernel, name='ffn_backward', out_shape=(pltpu.VMEM((ROWS,...  49.7 us
    pallas_call x1, Pallas kernels, body(): pl.pallas_call(functools.partial(finish, factor), name='finish', out_shap...  1.09 us

profile of v9, /device:TPU:0, one launch (start us, length us, event | category | flops | bytes accessed | tf_op | source)
XLA Modules:
  0.0 51.4 jit_solution(7710540638835833199)
XLA Ops:
  0.6 49.7 %ffn_backward.1 = (bf16[96,1024]{1,0:T(8,128)(2,1)S(1)}, bf16[1088,256]{1,0:T(8,128)(2,1)S(1)}) custom-call(bf16[96,1024]{1,0:T(8,128)(2,1)} %x_hbm.1, bf16[96,1024]{1,0:T(8,128)(2,1)} %o_hbm.1, bf16[352,256]{1,0:T(8,128)(2,1)} %bitcast.4, bf16[352,256]{1,0:T(8,128)(2,1)} %bitcast.5, bf16[352,256]{1,0:T(8,128)(2,1)} %d_hbm.1), custom_call_target="tpu_custom_call" | custom-call | tf_op jit(solution)/shard_map/ffn_backward/pallas_call | solution.py:454
  50.4 1.1 %finish.1 = (bf16[96,1024]{1,0:T(8,128)(2,1)}, f32[352,256]{1,0:T(8,128)}, f32[352,256]{1,0:T(8,128)}, f32[352,256]{1,0:T(8,128)}) custom-call(bf16[96,1024]{1,0:T(8,128)(2,1)S(1)} %get-tuple-element.10.gi_ref, bf16[1088,256]{1,0:T(8,128)(2,1)S(1)} %get-tuple-element.11.dw_ref), custom_call_target="tpu_custom_call" | custom-call | tf_op jit(solution)/shard_map/finish/pallas_call | solution.py:496
